TPU v7x, 512 devices: a 4x2x32 block of a 4x8x32 slice. The times are simulated.
512 devices in a mesh: grp: 2 (over y), sp: 64 (over z, core), tp: 4 (over x).
Axes of the slice: x: 4, y: 2, z: 32, core: 2. Of those that a mesh axis runs over, the one named last changes fastest.
The devices are a block of a 4x8x32 slice.
Arguments:
- tokens: bfloat16 [131072, 2048], P(('grp', 'sp', 'tp')), parts along dimension 0, may hold values from -6 to 6
- step: float32 [131072], P(('grp', 'sp')), parts along dimension 0, may hold values from 0.2 to 3.75
- in_gain: float32 [2048], replicated, may hold values from 0.1 to 1.9
- in_proj: bfloat16 [2048, 512], P(None, 'tp'), may hold values from -0.125 to 0.125
- decay_rate: float32 [32, 64], P('tp'), may hold values from 1.5258789e-06 to 0.04
- frequency: float32 [32, 64], P('tp'), may hold values from 0.2 to 3
- input_map: float32 [2, 32, 64, 16], P(None, 'tp'), may hold values from -1 to 1
- readout: float32 [2, 32, 16, 64], P(None, 'tp'), may hold values from -0.75 to 0.75
- out_gain: float32 [512], replicated, may hold values from 0.1 to 1.9
- out_proj: bfloat16 [512, 2048], replicated, may hold values from -0.25 to 0.25
Outputs:
- mixed: bfloat16 [131072, 2048], P(('grp', 'sp', 'tp')), parts along dimension 0
There are 2 independent parts, one for each index of `grp`. A program takes and returns all parts, laid end to end along the dimension named above; an argument that names none is the same for every part. Nothing has to cross between parts.
All inputs are finite; a program needn't handle non-finite values.
Results may differ from a plain program's by a relative error of at most 0.01.
Values may be sent and summed in bfloat16 or wider, within the bound.
A program may use at most 64 MiB of HBM per device.

v0:
```python
from functools import partial

import jax
import jax.numpy as jnp
from jax import lax
from jax.sharding import PartitionSpec as P

SPAN = 64


HIGHEST = lax.Precision.HIGHEST


def gathered_once(array, axis):
    leaves = jax.tree.leaves(array)
    sequence = sorted(range(len(leaves)), key=lambda k: -leaves[k].size)
    width = (1, *leaves[sequence[0]].shape)[-1]
    lines = [
        jnp.pad(leaves[k].reshape(-1), (0, -leaves[k].size % width)).reshape(-1, width)
        for k in sequence
    ]
    both, at, found = (lax.all_gather(jnp.concatenate(lines), axis), 0, {})
    for k, line in zip(sequence, lines):
        section = both[:, at : at + len(line)].reshape(len(both), -1)
        found[k] = section[:, : leaves[k].size].reshape(-1, *leaves[k].shape)
        at += len(line)
    numbers = iter(range(len(leaves)))
    return jax.tree.map(lambda _: found[next(numbers)], array)


def entering(value, axis, join, neutral):
    count, mine = (lax.axis_size(axis), lax.axis_index(axis))
    pieces = gathered_once(value, axis)
    so_far = jax.tree.map(
        lambda part, zero: jnp.full_like(part, 0) + jnp.asarray(zero, part.dtype), value, neutral
    )

    def lap(position, so_far):
        longer = join(so_far, jax.tree.map(lambda part: part[position], pieces))
        return jax.tree.map(lambda new, old: jnp.where(position < mine, new, old), longer, so_far)

    return lax.fori_loop(0, count - 1, lap, so_far)


def compose(earlier, later):
    a_re, a_im, b_re, b_im = earlier
    c_re, c_im, d_re, d_im = later
    return (
        c_re * a_re - c_im * a_im,
        c_re * a_im + c_im * a_re,
        c_re * b_re - c_im * b_im + d_re,
        c_re * b_im + c_im * b_re + d_im,
    )


def rms_rows(values, gain):
    values = values.astype(jnp.float32)
    scaled = values * lax.rsqrt(jnp.mean(values * values, axis=-1, keepdims=True) + 1e-06)
    return (scaled * gain).astype(jnp.bfloat16)


def block_tables(input_map, readout):
    groups = input_map.shape[1]
    unit = jnp.eye(groups, dtype=jnp.float32)
    push_re = jnp.einsum("gph,gk->ghkp", input_map[0], unit, precision=HIGHEST)
    push_im = jnp.einsum("gph,gk->ghkp", input_map[1], unit, precision=HIGHEST)
    read_re = jnp.einsum("ghp,gk->gpkh", readout[0], unit, precision=HIGHEST)
    read_im = jnp.einsum("ghp,gk->gpkh", readout[1], unit, precision=HIGHEST)
    inner = push_re.shape[0] * push_re.shape[1]
    flat = push_re.shape[2] * push_re.shape[3]
    return (
        push_re.reshape(inner, flat),
        push_im.reshape(inner, flat),
        read_re.reshape(flat, inner),
        read_im.reshape(flat, inner),
    )


def response(s_re, s_im, read_re, read_im):
    value = jnp.dot(s_re, read_re, precision=HIGHEST) - jnp.dot(s_im, read_im, precision=HIGHEST)
    return jax.nn.gelu(value, approximate=True).astype(jnp.bfloat16)


def advance(carry, piece, rates, freqs, tables, lower, keep):
    drive_part, time_part = piece
    push_re, push_im, read_re, read_im = tables
    own = time_part[:, None]
    magnitude = jnp.exp(-rates[None] * own)
    a_re = magnitude * jnp.cos(freqs[None] * own)
    a_im = magnitude * jnp.sin(freqs[None] * own)
    lam_re = -rates
    denom = lam_re * lam_re + freqs * freqs
    n_re = a_re - 1.0
    z_re = (n_re * lam_re + a_im * freqs) / denom
    z_im = (a_im * lam_re - n_re * freqs) / denom
    grouped = drive_part.astype(jnp.float32)
    in_re = jnp.dot(grouped, push_re, precision=HIGHEST)
    in_im = jnp.dot(grouped, push_im, precision=HIGHEST)
    i_re = z_re * in_re - z_im * in_im
    i_im = z_re * in_im + z_im * in_re
    elapsed = jnp.dot(lower, time_part, precision=HIGHEST)[:, None]
    grow = jnp.exp(rates[None] * elapsed)
    angle = freqs[None] * elapsed
    cosine = jnp.cos(angle)
    sine = jnp.sin(angle)
    w_re = grow * (cosine * i_re + sine * i_im)
    w_im = grow * (cosine * i_im - sine * i_re)
    acc_re = jnp.dot(lower, w_re, precision=HIGHEST)
    acc_im = jnp.dot(lower, w_im, precision=HIGHEST)
    shrink = jnp.exp(-rates[None] * elapsed)
    c_re = shrink * cosine
    c_im = shrink * sine
    s_re = c_re * acc_re - c_im * acc_im
    s_im = c_re * acc_im + c_im * acc_re
    d_re, d_im, e_re, e_im = carry
    full_re = s_re + c_re * e_re - c_im * e_im
    full_im = s_im + c_re * e_im + c_im * e_re
    cum_re = c_re * d_re - c_im * d_im
    cum_im = c_re * d_im + c_im * d_re
    ends = (cum_re[-1], cum_im[-1], full_re[-1], full_im[-1])
    return (ends, (cum_re, cum_im, full_re, full_im))


def on_device(
    tokens, step, in_gain, in_proj, decay_rate, frequency, input_map, readout, out_gain, out_proj
):
    normed = rms_rows(tokens, in_gain)
    rates, freqs, maps, reads = (decay_rate, frequency, input_map, readout)
    drive = jnp.dot(
        lax.all_gather(normed, "tp", axis=0, tiled=True),
        in_proj,
        preferred_element_type=jnp.float32,
    ).astype(jnp.bfloat16)
    tables = block_tables(maps, reads)
    flat_rates = rates.reshape(-1)
    flat_freqs = freqs.reshape(-1)
    seq_rows = drive.shape[0]
    block_count = seq_rows // SPAN
    drive_blocks = drive.reshape(block_count, SPAN, -1)
    time_blocks = step.reshape(block_count, SPAN)
    rows_index = lax.broadcasted_iota(jnp.int32, (SPAN, SPAN), 0)
    cols_index = lax.broadcasted_iota(jnp.int32, (SPAN, SPAN), 1)
    lower = (cols_index <= rows_index).astype(jnp.float32)
    zeros = jnp.zeros(flat_rates.shape, jnp.float32)
    ones = jnp.ones(flat_rates.shape, jnp.float32)
    start_carry = (ones, zeros, zeros, zeros)
    keep_first = "states"
    ends, stored = lax.scan(
        partial(
            advance, rates=flat_rates, freqs=flat_freqs, tables=tables, lower=lower, keep=keep_first
        ),
        start_carry,
        (drive_blocks, time_blocks),
    )
    incoming = entering(ends, "sp", compose, start_carry)
    cum_re, cum_im, full_re, full_im = stored
    width = flat_rates.shape[0]
    cum_re = cum_re.reshape(seq_rows, width)
    cum_im = cum_im.reshape(seq_rows, width)
    state_re = full_re.reshape(seq_rows, width) + cum_re * incoming[2] - cum_im * incoming[3]
    state_im = full_im.reshape(seq_rows, width) + cum_re * incoming[3] + cum_im * incoming[2]
    answer = response(state_re, state_im, tables[2], tables[3])
    gathered = lax.all_to_all(answer, "tp", split_axis=0, concat_axis=1, tiled=True)
    shaped = rms_rows(gathered, out_gain)
    return jnp.dot(shaped, out_proj, preferred_element_type=jnp.float32).astype(jnp.bfloat16)


def solution(mesh):
    placed = (
        P(("grp", "sp", "tp"), None),
        P(("grp", "sp")),
        P(),
        P(None, "tp"),
        P("tp", None),
        P("tp", None),
        P(None, "tp", None, None),
        P(None, "tp", None, None),
        P(),
        P(),
    )
    return jax.shard_map(
        on_device,
        mesh=mesh,
        in_specs=placed,
        out_specs=P(("grp", "sp", "tp"), None),
        check_vma=False,
    )
```

profile of v0, /device:TPU:33, one launch (start us, length us, event | category | flops | bytes accessed | tf_op | source)
XLA Modules:
  0.0 373.2 jit_solution(620879934638658215)
XLA Ops:
  6.6 1.7 fusion.44
  8.3 2.5 fusion.46
  15.7 85.1 %all-gather.4.cloned.1.call-done = bf16[1024,2048]{1,0:T(8,128)(2,1)} async-done(((bf16[256,2048]{1,0:T(8,128)(2,1)}), bf16[1024,2048]{1,0:T(8,128)(2,1)}) %all-gather.4.cloned.1.call-update) | async-done | bytes 4194320 | tf_op jit(solution)/shard_map/all_gather | solution.py:130
  100.8 4.3 %convolution_convert_fusion.1 = bf16[1024,128]{1,0:T(8,128)(2,1)} fusion(bf16[1024,2048]{1,0:T(8,128)(2,1)} %all-gather.4.cloned.1.call-done, bf16[2048,128]{1,0:T(8,128)(2,1)} %param.17), kind=kOutput, calls=%fused_computation.81 | convolution fusion | flops 537001984 | bytes 4980736 | tf_op jit(solution)/shard_map/dot_general | solution.py:129
  106.2 173.9 %while.48 = (s32[]{:T(128)}, f32[512]{0:T(512)S(1)}, f32[512]{0:T(512)S(1)}, f32[512]{0:T(512)}, f32[512]{0:T(512)}, /*index=5*/f32[16,64,512]{2,1,0:T(8,128)}, ...) while((s32[]{:T(128)}, f32[512]{0:T(512)S(1)}, ...), condition=%wide.wide.region_2.3_spmd.clone.clone.clone, body=%wide.wide.region_1.2_spmd.clone.clone.clone.sunk | while | flops 153889792 | bytes 4405837 | solution.py:148
  106.6 1.0 fusion.103
  110.2 2.0 convolution_bitcast_fusion.8
  112.3 3.0 add_dynamic-update-slice_fusion.3
  117.4 1.0 fusion.103
  121.1 2.0 convolution_bitcast_fusion.8
  123.2 3.0 add_dynamic-update-slice_fusion.3
  128.3 1.0 fusion.103
  129.4 1.0 fusion.104
  131.9 2.0 convolution_bitcast_fusion.8
  134.1 3.0 add_dynamic-update-slice_fusion.3
  139.2 1.0 fusion.103
  140.3 1.0 fusion.104
  142.8 2.0 convolution_bitcast_fusion.8
  144.9 3.0 add_dynamic-update-slice_fusion.3
  150.1 1.0 fusion.103
  151.2 1.0 fusion.104
  153.7 2.0 convolution_bitcast_fusion.8
  155.8 3.0 add_dynamic-update-slice_fusion.3
  160.9 1.0 fusion.103
  162.1 1.0 fusion.104
  164.6 2.0 convolution_bitcast_fusion.8
  166.7 3.0 add_dynamic-update-slice_fusion.3
  171.8 1.0 fusion.103
  175.5 2.0 convolution_bitcast_fusion.8
  177.6 3.0 add_dynamic-update-slice_fusion.3
  183.8 1.0 fusion.104
  186.3 2.0 convolution_bitcast_fusion.8
  188.4 3.0 add_dynamic-update-slice_fusion.3
  193.6 1.0 fusion.103
  194.7 1.0 fusion.104
  197.2 2.0 convolution_bitcast_fusion.8
  199.3 3.0 add_dynamic-update-slice_fusion.3
  204.4 1.0 fusion.103
  208.1 2.0 convolution_bitcast_fusion.8
  210.2 3.0 add_dynamic-update-slice_fusion.3
  216.4 1.0 fusion.104
  218.9 2.0 convolution_bitcast_fusion.8
  221.0 3.0 add_dynamic-update-slice_fusion.3
  226.1 1.0 fusion.103
  227.3 1.0 fusion.104
  229.8 2.0 convolution_bitcast_fusion.8
  231.9 3.0 add_dynamic-update-slice_fusion.3
  238.1 1.0 fusion.104
  240.7 2.0 convolution_bitcast_fusion.8
  242.8 3.0 add_dynamic-update-slice_fusion.3
  251.5 2.0 convolution_bitcast_fusion.8
  253.6 3.0 add_dynamic-update-slice_fusion.3
  258.8 1.0 fusion.103
  262.4 2.0 convolution_bitcast_fusion.8
  264.5 3.0 add_dynamic-update-slice_fusion.3
  273.3 2.0 convolution_bitcast_fusion.8
  275.4 3.0 add_dynamic-update-slice_fusion.3
  280.9 60.4 %all-gather.1 = f32[64,4,512]{2,1,0:T(4,128)S(1)} all-gather(f32[1,4,512]{2,1,0:T(4,128)S(1)} %maximum_bitcast_fusion), channel_id=2, replica_groups=mesh['grp'=2,'sp'=64,'tp'=4] {'sp'}, dimensions={0}, use_global_device_ids=true | all-gather | bytes 532480 | tf_op jit(solution)/shard_map/all_gather | solution.py:22
  341.7 5.1 %while.47 = (s32[]{:T(128)}, f32[512]{0:T(512)S(1)}, f32[512]{0:T(512)S(1)}, s32[]{:T(128)}, f32[64,512]{1,0:T(8,128)S(1)}, /*index=5*/f32[64,512]{1,0:T(8,128)S...) while((s32[]{:T(128)}, f32[512]{0:T(512)S(1)}, f32[512]{0:T(512)S(1)}, ...), condition=%wide.region_4.5_spmd.clone, body=%wide.region_3.4_spmd.clone.sunk | while | flops 6148 | bytes 32897 | solution.py:42
  346.8 4.6 %multiply_add_fusion.5 = (f32[16,64,512]{2,1,0:T(8,128)S(1)}, f32[16,64,512]{2,1,0:T(8,128)S(1)}) fusion(f32[16,64,512]{2,1,0:T(8,128)} %get-tuple-element.435, f32[16,64,512]{2,1,0:T(8,128)} %get-tuple-element.437, f32[16,64,512]{2,1,0:T(8,128)} %get-tuple-element.429, f32[512]{0:T(512)S(1)} %get-tuple-element.436, f32[512]{0:T(512)S(1)} %get-tuple-element.434, ...), kind=kLoop, calls=%fused_computation.78 | loop fusion | flops 4194304 | bytes 12587008 | tf_op jit(solution)/shard_map/add | solution.py:161
  351.4 1.8 fusion.59
  353.3 1.8 fusion.54
  355.2 9.2 %all_to_all.13 = bf16[4,256,128]{1,2,0:T(8,128)(2,1)S(1)} all-to-all(bf16[4,256,128]{1,2,0:T(8,128)(2,1)S(1)} %copy.20), channel_id=1, replica_groups=mesh['grp'=2,'sp'=64,'tp'=4] {'tp'}, dimensions={0} | all-to-all | bytes 524288 | tf_op jit(solution)/shard_map/all_to_all | solution.py:163
  364.7 1.7 convolution_convert_fusion
  (595 shorter events, 81.8 us)
Async XLA Ops:
  6.5 358.1 %copy-start = (bf16[512,2048]{1,0:T(8,128)(2,1)S(1)}, bf16[512,2048]{1,0:T(8,128)(2,1)}, u32[]{:S(2)}) copy-start(bf16[512,2048]{1,0:T(8,128)(2,1)} %param.23) | copy-start | bytes 6291460
  6.6 6.4 %copy-start.12 = (f32[1024]{0:T(1024)S(1)}, f32[1024]{0:T(1024)}, u32[]{:S(2)}) copy-start(f32[1024]{0:T(1024)} %param.15) | copy-start | bytes 12292
  6.6 7.0 %copy-start.3 = (f32[2,8,16,64]{3,2,1,0:T(8,128)S(1)}, f32[2,8,16,64]{3,2,1,0:T(8,128)}, u32[]{:S(2)}) copy-start(f32[2,8,16,64]{3,2,1,0:T(8,128)} %param.21) | copy-start | bytes 196612
  6.6 94.2 %all-gather.4.cloned.1.call-start = ((), (), s32[]{:S(2)}) async-start(), calls=%async_computation.1 | async-start | bytes 5242880 | tf_op jit(solution)/shard_map/all_gather | solution.py:130
  106.5 5.7 %copy-start.5 = (f32[1,512]{1,0:T(1,128)S(1)}, f32[1,512]{1,0:T(1,128)}, u32[]{:S(2)}) copy-start(f32[1,512]{1,0:T(1,128)} %get-tuple-element.1028) | copy-start | bytes 6148 | tf_op jit(solution)/shard_map/while
  106.5 5.7 %copy-start.10 = (f32[512]{0:T(512)S(1)}, f32[512]{0:T(512)}, u32[]{:S(2)}) copy-start(f32[512]{0:T(512)} %get-tuple-element.1001) | copy-start | bytes 6148 | tf_op jit(solution)/shard_map/while
  106.5 5.7 %copy-start.11 = (f32[512]{0:T(512)S(1)}, f32[512]{0:T(512)}, u32[]{:S(2)}) copy-start(f32[512]{0:T(512)} %get-tuple-element.1002) | copy-start | bytes 6148 | tf_op jit(solution)/shard_map/while
  106.5 5.7 %copy-start.14 = (f32[512]{0:T(512)S(1)}, f32[512]{0:T(512)}, u32[]{:S(2)}) copy-start(f32[512]{0:T(512)} %get-tuple-element.1038) | copy-start | bytes 6148 | tf_op jit(solution)/shard_map/while
  106.6 5.7 %copy-start.15 = (f32[1,512]{1,0:T(1,128)S(1)}, f32[1,512]{1,0:T(1,128)}, u32[]{:S(2)}) copy-start(f32[1,512]{1,0:T(1,128)} %get-tuple-element.1032) | copy-start | bytes 6148 | tf_op jit(solution)/shard_map/while
  117.4 5.7 %copy-start.5 = (f32[1,512]{1,0:T(1,128)S(1)}, f32[1,512]{1,0:T(1,128)}, u32[]{:S(2)}) copy-start(f32[1,512]{1,0:T(1,128)} %get-tuple-element.1028) | copy-start | bytes 6148 | tf_op jit(solution)/shard_map/while
  117.4 5.7 %copy-start.10 = (f32[512]{0:T(512)S(1)}, f32[512]{0:T(512)}, u32[]{:S(2)}) copy-start(f32[512]{0:T(512)} %get-tuple-element.1001) | copy-start | bytes 6148 | tf_op jit(solution)/shard_map/while
  128.3 5.7 %copy-start.5 = (f32[1,512]{1,0:T(1,128)S(1)}, f32[1,512]{1,0:T(1,128)}, u32[]{:S(2)}) copy-start(f32[1,512]{1,0:T(1,128)} %get-tuple-element.1028) | copy-start | bytes 6148 | tf_op jit(solution)/shard_map/while
  128.3 5.7 %copy-start.10 = (f32[512]{0:T(512)S(1)}, f32[512]{0:T(512)}, u32[]{:S(2)}) copy-start(f32[512]{0:T(512)} %get-tuple-element.1001) | copy-start | bytes 6148 | tf_op jit(solution)/shard_map/while
  128.3 5.7 %copy-start.11 = (f32[512]{0:T(512)S(1)}, f32[512]{0:T(512)}, u32[]{:S(2)}) copy-start(f32[512]{0:T(512)} %get-tuple-element.1002) | copy-start | bytes 6148 | tf_op jit(solution)/shard_map/while
  128.3 5.7 %copy-start.14 = (f32[512]{0:T(512)S(1)}, f32[512]{0:T(512)}, u32[]{:S(2)}) copy-start(f32[512]{0:T(512)} %get-tuple-element.1038) | copy-start | bytes 6148 | tf_op jit(solution)/shard_map/while
  128.3 5.7 %copy-start.15 = (f32[1,512]{1,0:T(1,128)S(1)}, f32[1,512]{1,0:T(1,128)}, u32[]{:S(2)}) copy-start(f32[1,512]{1,0:T(1,128)} %get-tuple-element.1032) | copy-start | bytes 6148 | tf_op jit(solution)/shard_map/while
  139.1 5.7 %copy-start.5 = (f32[1,512]{1,0:T(1,128)S(1)}, f32[1,512]{1,0:T(1,128)}, u32[]{:S(2)}) copy-start(f32[1,512]{1,0:T(1,128)} %get-tuple-element.1028) | copy-start | bytes 6148 | tf_op jit(solution)/shard_map/while
  139.2 5.7 %copy-start.10 = (f32[512]{0:T(512)S(1)}, f32[512]{0:T(512)}, u32[]{:S(2)}) copy-start(f32[512]{0:T(512)} %get-tuple-element.1001) | copy-start | bytes 6148 | tf_op jit(solution)/shard_map/while
  139.2 5.7 %copy-start.11 = (f32[512]{0:T(512)S(1)}, f32[512]{0:T(512)}, u32[]{:S(2)}) copy-start(f32[512]{0:T(512)} %get-tuple-element.1002) | copy-start | bytes 6148 | tf_op jit(solution)/shard_map/while
  139.2 5.7 %copy-start.14 = (f32[512]{0:T(512)S(1)}, f32[512]{0:T(512)}, u32[]{:S(2)}) copy-start(f32[512]{0:T(512)} %get-tuple-element.1038) | copy-start | bytes 6148 | tf_op jit(solution)/shard_map/while
  139.2 5.7 %copy-start.15 = (f32[1,512]{1,0:T(1,128)S(1)}, f32[1,512]{1,0:T(1,128)}, u32[]{:S(2)}) copy-start(f32[1,512]{1,0:T(1,128)} %get-tuple-element.1032) | copy-start | bytes 6148 | tf_op jit(solution)/shard_map/while
  150.0 5.7 %copy-start.5 = (f32[1,512]{1,0:T(1,128)S(1)}, f32[1,512]{1,0:T(1,128)}, u32[]{:S(2)}) copy-start(f32[1,512]{1,0:T(1,128)} %get-tuple-element.1028) | copy-start | bytes 6148 | tf_op jit(solution)/shard_map/while
  150.0 5.7 %copy-start.10 = (f32[512]{0:T(512)S(1)}, f32[512]{0:T(512)}, u32[]{:S(2)}) copy-start(f32[512]{0:T(512)} %get-tuple-element.1001) | copy-start | bytes 6148 | tf_op jit(solution)/shard_map/while
  150.0 5.7 %copy-start.11 = (f32[512]{0:T(512)S(1)}, f32[512]{0:T(512)}, u32[]{:S(2)}) copy-start(f32[512]{0:T(512)} %get-tuple-element.1002) | copy-start | bytes 6148 | tf_op jit(solution)/shard_map/while
  150.0 5.7 %copy-start.14 = (f32[512]{0:T(512)S(1)}, f32[512]{0:T(512)}, u32[]{:S(2)}) copy-start(f32[512]{0:T(512)} %get-tuple-element.1038) | copy-start | bytes 6148 | tf_op jit(solution)/shard_map/while
  150.1 5.7 %copy-start.15 = (f32[1,512]{1,0:T(1,128)S(1)}, f32[1,512]{1,0:T(1,128)}, u32[]{:S(2)}) copy-start(f32[1,512]{1,0:T(1,128)} %get-tuple-element.1032) | copy-start | bytes 6148 | tf_op jit(solution)/shard_map/while
  160.9 5.7 %copy-start.5 = (f32[1,512]{1,0:T(1,128)S(1)}, f32[1,512]{1,0:T(1,128)}, u32[]{:S(2)}) copy-start(f32[1,512]{1,0:T(1,128)} %get-tuple-element.1028) | copy-start | bytes 6148 | tf_op jit(solution)/shard_map/while
  160.9 5.7 %copy-start.10 = (f32[512]{0:T(512)S(1)}, f32[512]{0:T(512)}, u32[]{:S(2)}) copy-start(f32[512]{0:T(512)} %get-tuple-element.1001) | copy-start | bytes 6148 | tf_op jit(solution)/shard_map/while
  160.9 5.7 %copy-start.11 = (f32[512]{0:T(512)S(1)}, f32[512]{0:T(512)}, u32[]{:S(2)}) copy-start(f32[512]{0:T(512)} %get-tuple-element.1002) | copy-start | bytes 6148 | tf_op jit(solution)/shard_map/while
  160.9 5.7 %copy-start.14 = (f32[512]{0:T(512)S(1)}, f32[512]{0:T(512)}, u32[]{:S(2)}) copy-start(f32[512]{0:T(512)} %get-tuple-element.1038) | copy-start | bytes 6148 | tf_op jit(solution)/shard_map/while
  160.9 5.7 %copy-start.15 = (f32[1,512]{1,0:T(1,128)S(1)}, f32[1,512]{1,0:T(1,128)}, u32[]{:S(2)}) copy-start(f32[1,512]{1,0:T(1,128)} %get-tuple-element.1032) | copy-start | bytes 6148 | tf_op jit(solution)/shard_map/while
  171.8 5.7 %copy-start.5 = (f32[1,512]{1,0:T(1,128)S(1)}, f32[1,512]{1,0:T(1,128)}, u32[]{:S(2)}) copy-start(f32[1,512]{1,0:T(1,128)} %get-tuple-element.1028) | copy-start | bytes 6148 | tf_op jit(solution)/shard_map/while
  171.8 5.7 %copy-start.10 = (f32[512]{0:T(512)S(1)}, f32[512]{0:T(512)}, u32[]{:S(2)}) copy-start(f32[512]{0:T(512)} %get-tuple-element.1001) | copy-start | bytes 6148 | tf_op jit(solution)/shard_map/while
  171.8 5.7 %copy-start.11 = (f32[512]{0:T(512)S(1)}, f32[512]{0:T(512)}, u32[]{:S(2)}) copy-start(f32[512]{0:T(512)} %get-tuple-element.1002) | copy-start | bytes 6148 | tf_op jit(solution)/shard_map/while
  171.8 5.7 %copy-start.14 = (f32[512]{0:T(512)S(1)}, f32[512]{0:T(512)}, u32[]{:S(2)}) copy-start(f32[512]{0:T(512)} %get-tuple-element.1038) | copy-start | bytes 6148 | tf_op jit(solution)/shard_map/while
  171.8 5.7 %copy-start.15 = (f32[1,512]{1,0:T(1,128)S(1)}, f32[1,512]{1,0:T(1,128)}, u32[]{:S(2)}) copy-start(f32[1,512]{1,0:T(1,128)} %get-tuple-element.1032) | copy-start | bytes 6148 | tf_op jit(solution)/shard_map/while
  182.6 5.7 %copy-start.5 = (f32[1,512]{1,0:T(1,128)S(1)}, f32[1,512]{1,0:T(1,128)}, u32[]{:S(2)}) copy-start(f32[1,512]{1,0:T(1,128)} %get-tuple-element.1028) | copy-start | bytes 6148 | tf_op jit(solution)/shard_map/while
  182.6 5.7 %copy-start.10 = (f32[512]{0:T(512)S(1)}, f32[512]{0:T(512)}, u32[]{:S(2)}) copy-start(f32[512]{0:T(512)} %get-tuple-element.1001) | copy-start | bytes 6148 | tf_op jit(solution)/shard_map/while
  182.7 5.7 %copy-start.11 = (f32[512]{0:T(512)S(1)}, f32[512]{0:T(512)}, u32[]{:S(2)}) copy-start(f32[512]{0:T(512)} %get-tuple-element.1002) | copy-start | bytes 6148 | tf_op jit(solution)/shard_map/while
  182.7 5.7 %copy-start.14 = (f32[512]{0:T(512)S(1)}, f32[512]{0:T(512)}, u32[]{:S(2)}) copy-start(f32[512]{0:T(512)} %get-tuple-element.1038) | copy-start | bytes 6148 | tf_op jit(solution)/shard_map/while
  182.7 5.7 %copy-start.15 = (f32[1,512]{1,0:T(1,128)S(1)}, f32[1,512]{1,0:T(1,128)}, u32[]{:S(2)}) copy-start(f32[1,512]{1,0:T(1,128)} %get-tuple-element.1032) | copy-start | bytes 6148 | tf_op jit(solution)/shard_map/while
  193.5 5.7 %copy-start.5 = (f32[1,512]{1,0:T(1,128)S(1)}, f32[1,512]{1,0:T(1,128)}, u32[]{:S(2)}) copy-start(f32[1,512]{1,0:T(1,128)} %get-tuple-element.1028) | copy-start | bytes 6148 | tf_op jit(solution)/shard_map/while
  193.5 5.7 %copy-start.10 = (f32[512]{0:T(512)S(1)}, f32[512]{0:T(512)}, u32[]{:S(2)}) copy-start(f32[512]{0:T(512)} %get-tuple-element.1001) | copy-start | bytes 6148 | tf_op jit(solution)/shard_map/while
  193.5 5.7 %copy-start.11 = (f32[512]{0:T(512)S(1)}, f32[512]{0:T(512)}, u32[]{:S(2)}) copy-start(f32[512]{0:T(512)} %get-tuple-element.1002) | copy-start | bytes 6148 | tf_op jit(solution)/shard_map/while
  193.5 5.7 %copy-start.14 = (f32[512]{0:T(512)S(1)}, f32[512]{0:T(512)}, u32[]{:S(2)}) copy-start(f32[512]{0:T(512)} %get-tuple-element.1038) | copy-start | bytes 6148 | tf_op jit(solution)/shard_map/while
  193.5 5.7 %copy-start.15 = (f32[1,512]{1,0:T(1,128)S(1)}, f32[1,512]{1,0:T(1,128)}, u32[]{:S(2)}) copy-start(f32[1,512]{1,0:T(1,128)} %get-tuple-element.1032) | copy-start | bytes 6148 | tf_op jit(solution)/shard_map/while
  226.1 5.7 %copy-start.5 = (f32[1,512]{1,0:T(1,128)S(1)}, f32[1,512]{1,0:T(1,128)}, u32[]{:S(2)}) copy-start(f32[1,512]{1,0:T(1,128)} %get-tuple-element.1028) | copy-start | bytes 6148 | tf_op jit(solution)/shard_map/while
  226.1 5.7 %copy-start.10 = (f32[512]{0:T(512)S(1)}, f32[512]{0:T(512)}, u32[]{:S(2)}) copy-start(f32[512]{0:T(512)} %get-tuple-element.1001) | copy-start | bytes 6148 | tf_op jit(solution)/shard_map/while
  226.1 5.7 %copy-start.11 = (f32[512]{0:T(512)S(1)}, f32[512]{0:T(512)}, u32[]{:S(2)}) copy-start(f32[512]{0:T(512)} %get-tuple-element.1002) | copy-start | bytes 6148 | tf_op jit(solution)/shard_map/while
  226.1 5.7 %copy-start.14 = (f32[512]{0:T(512)S(1)}, f32[512]{0:T(512)}, u32[]{:S(2)}) copy-start(f32[512]{0:T(512)} %get-tuple-element.1038) | copy-start | bytes 6148 | tf_op jit(solution)/shard_map/while
  226.1 5.7 %copy-start.15 = (f32[1,512]{1,0:T(1,128)S(1)}, f32[1,512]{1,0:T(1,128)}, u32[]{:S(2)}) copy-start(f32[1,512]{1,0:T(1,128)} %get-tuple-element.1032) | copy-start | bytes 6148 | tf_op jit(solution)/shard_map/while
  237.0 5.7 %copy-start.5 = (f32[1,512]{1,0:T(1,128)S(1)}, f32[1,512]{1,0:T(1,128)}, u32[]{:S(2)}) copy-start(f32[1,512]{1,0:T(1,128)} %get-tuple-element.1028) | copy-start | bytes 6148 | tf_op jit(solution)/shard_map/while
  237.0 5.7 %copy-start.10 = (f32[512]{0:T(512)S(1)}, f32[512]{0:T(512)}, u32[]{:S(2)}) copy-start(f32[512]{0:T(512)} %get-tuple-element.1001) | copy-start | bytes 6148 | tf_op jit(solution)/shard_map/while
  237.0 5.7 %copy-start.11 = (f32[512]{0:T(512)S(1)}, f32[512]{0:T(512)}, u32[]{:S(2)}) copy-start(f32[512]{0:T(512)} %get-tuple-element.1002) | copy-start | bytes 6148 | tf_op jit(solution)/shard_map/while
  237.0 5.7 %copy-start.14 = (f32[512]{0:T(512)S(1)}, f32[512]{0:T(512)}, u32[]{:S(2)}) copy-start(f32[512]{0:T(512)} %get-tuple-element.1038) | copy-start | bytes 6148 | tf_op jit(solution)/shard_map/while
  237.0 5.7 %copy-start.15 = (f32[1,512]{1,0:T(1,128)S(1)}, f32[1,512]{1,0:T(1,128)}, u32[]{:S(2)}) copy-start(f32[1,512]{1,0:T(1,128)} %get-tuple-element.1032) | copy-start | bytes 6148 | tf_op jit(solution)/shard_map/while
  258.7 5.7 %copy-start.5 = (f32[1,512]{1,0:T(1,128)S(1)}, f32[1,512]{1,0:T(1,128)}, u32[]{:S(2)}) copy-start(f32[1,512]{1,0:T(1,128)} %get-tuple-element.1028) | copy-start | bytes 6148 | tf_op jit(solution)/shard_map/while
  258.7 5.7 %copy-start.10 = (f32[512]{0:T(512)S(1)}, f32[512]{0:T(512)}, u32[]{:S(2)}) copy-start(f32[512]{0:T(512)} %get-tuple-element.1001) | copy-start | bytes 6148 | tf_op jit(solution)/shard_map/while
  258.7 5.7 %copy-start.11 = (f32[512]{0:T(512)S(1)}, f32[512]{0:T(512)}, u32[]{:S(2)}) copy-start(f32[512]{0:T(512)} %get-tuple-element.1002) | copy-start | bytes 6148 | tf_op jit(solution)/shard_map/while
  258.7 5.7 %copy-start.14 = (f32[512]{0:T(512)S(1)}, f32[512]{0:T(512)}, u32[]{:S(2)}) copy-start(f32[512]{0:T(512)} %get-tuple-element.1038) | copy-start | bytes 6148 | tf_op jit(solution)/shard_map/while
  258.8 5.7 %copy-start.15 = (f32[1,512]{1,0:T(1,128)S(1)}, f32[1,512]{1,0:T(1,128)}, u32[]{:S(2)}) copy-start(f32[1,512]{1,0:T(1,128)} %get-tuple-element.1032) | copy-start | bytes 6148 | tf_op jit(solution)/shard_map/while
  280.2 61.5 %copy-start.6 = (f32[512]{0:T(512)S(1)}, f32[512]{0:T(512)}, u32[]{:S(2)}) copy-start(f32[512]{0:T(512)} %custom-call) | copy-start | bytes 6148
  280.2 61.5 %copy-start.7 = (f32[512]{0:T(512)S(1)}, f32[512]{0:T(512)}, u32[]{:S(2)}) copy-start(f32[512]{0:T(512)} %custom-call.1) | copy-start | bytes 6148
  353.2 11.3 %copy-start.13 = (f32[512]{0:T(512)S(1)}, f32[512]{0:T(512)}, u32[]{:S(2)}) copy-start(f32[512]{0:T(512)} %param.22) | copy-start | bytes 6148
  (28 other events, 152.0 us)
Sparse Core Ops, SparseCore 0:
  11.0 89.7 all-gather.3
where the time goes:
time: 378 us; the launch traced here: 373 us
  matrix products  134 us (35%)
  waiting for transfers between devices  85.1 us (23%)
  blocking collectives  69.5 us (18%)
  local copies, waits for them, and re-layouts  43.1 us (11%)
  other arithmetic  22.5 us (6%)
  between operations  13.7 us (4%)
  loops' own time  5.22 us (1%)
    all_gather x1, waiting for transfers between devices, on_device(): lax.all_gather(normed, 'tp', axis=0, tiled=True)  85.1 us
    all_gather x1, blocking collectives, gathered_once(): both, at, found = (lax.all_gather(jnp.concatenate(lines), axis), 0, {})  60.4 us
    dot_general x16, matrix products, advance(): acc_im = jnp.dot(lower, w_im, precision=HIGHEST)  48.1 us
    dot_general x16, matrix products, advance(): acc_re = jnp.dot(lower, w_re, precision=HIGHEST)  32.4 us
    slice x32, local copies, waits for them, and re-layouts, advance(): ends = (cum_re[-1], cum_im[-1], full_re[-1], full_im[-1])  18.8 us
    dot_general x16, matrix products, advance(): in_im = jnp.dot(grouped, push_im, precision=HIGHEST)  15.3 us
    dot_general x16, matrix products, advance(): in_re = jnp.dot(grouped, push_re, precision=HIGHEST)  15.3 us
    dot_general x16, matrix products, advance(): elapsed = jnp.dot(lower, time_part, precision=HIGHEST)[:, None]  13.3 us
  transfers between devices with their start and end apart: 1, of which 1 were waited for; matrix products, arithmetic and copies ran while one was open for 1% of the time, Pallas kernels for 0%

commit v1 on v0

v1 whole, which is shorter than its diff:
```python
import functools

import jax
import jax.numpy as jnp
import numpy as np
from jax import lax
from jax.experimental import pallas as pl
from jax.experimental.pallas import tpu as pltpu
from jax.sharding import PartitionSpec as P

F32, BF16 = jnp.float32, jnp.bfloat16
MESH = pl.DeviceIdType.MESH
LANES = 128
CHUNK = 64
SIN = (6.283182782944718, -41.34141729070845, 81.59606953187966, -76.57887013158442, 41.19977042473147, -12.262090350994187)
COS = (0.9999999888727491, -19.7392044313539, 64.939113609812, -85.45006239525888, 60.16694808625918, -25.96486025322117, 6.5245930831162795)
TURN = np.float32(1.0 / (2.0 * np.pi))
TURN_LOW = np.float32(1.0 / (2.0 * np.pi) - float(TURN))


def halves(value):
    wide = value * np.float32(4097.0)
    high = wide - (wide - value)
    return high, value - high


def turns_of(freqs):
    high = freqs * TURN
    f_high, f_low = halves(freqs)
    c_high, c_low = (np.float32(v) for v in halves(TURN))
    error = ((f_high * c_high - high) + f_high * c_low + f_low * c_high) + f_low * c_low
    return high, error + freqs * TURN_LOW


def polynomial(x, terms):
    total = jnp.full_like(x, np.float32(terms[-1]))
    for term in terms[-2::-1]:
        total = total * x + np.float32(term)
    return total


def rotation(high, low, times):
    whole = high * times
    part = (whole - jnp.round(whole)) + low * times
    square = part * part
    return polynomial(square, COS), polynomial(square, SIN) * part


def gather_kernel(
    proj, tables, rates, step, all_proj, all_tables, all_rates, both_steps,
    proj_own, tables_own, rates_own, step_own, send, recv, small_send, small_recv, local,
):
    count = lax.axis_size("tp")
    me, sp = lax.axis_index("tp"), lax.axis_index("sp")
    core = lax.rem(sp, 2)
    partner = {"sp": sp + 1 - 2 * core}
    right, left = lax.rem(me + 1, count), lax.rem(me + count - 1, count)
    across = lax.rem(me + 2, count)
    to_right, to_left, to_across = {"tp": right}, {"tp": left}, {"tp": across}

    barrier = pltpu.get_barrier_semaphore()
    for target in (to_right, to_left, to_across, partner):
        pl.semaphore_signal(barrier, inc=1, device_id=target, device_id_type=MESH)

    inward = [
        pltpu.make_async_copy(src, dst, local.at[k])
        for k, (src, dst) in enumerate(
            ((proj, proj_own), (tables, tables_own), (rates, rates_own), (step, step_own))
        )
    ]
    for copy in inward:
        copy.start()
    for copy in inward:
        copy.wait()
    pl.semaphore_wait(barrier, 4)

    pairs = ((proj_own, all_proj), (tables_own, all_tables))

    def rows(k, quarter):
        quarter_rows = pairs[k][0].shape[0] // 4
        return pl.ds(pl.multiple_of((core * 2 + quarter) * quarter_rows, quarter_rows), quarter_rows)

    def remote(src, dst, slot, target):
        return pltpu.make_async_remote_copy(
            src_ref=src, dst_ref=dst, send_sem=send.at[slot], recv_sem=recv.at[slot],
            device_id=target, device_id_type=MESH,
        )

    def piece(k, shard, quarter, slot, target, own=False):
        own_ref, all_ref = pairs[k]
        where = rows(k, quarter)
        dst = all_ref.at[shard, where]
        return remote(own_ref.at[where] if own else dst, dst, slot, target)

    started = []

    def go(copy):
        copy.start()
        started.append(copy)

    for order in range(2):
        for k in (1, 0):
            go(piece(k, me, order, k * 12 + order, to_right, own=True))
            go(piece(k, me, 1 - order, k * 12 + 2 + order, to_left, own=True))
    small = []
    for slot, target in enumerate((to_right, to_left, to_across)):
        small.append(
            pltpu.make_async_remote_copy(
                src_ref=rates_own, dst_ref=all_rates.at[me], send_sem=small_send.at[slot],
                recv_sem=small_recv.at[slot], device_id=target, device_id_type=MESH,
            )
        )
    small.append(
        pltpu.make_async_remote_copy(
            src_ref=step_own, dst_ref=both_steps.at[core], send_sem=small_send.at[3],
            recv_sem=small_recv.at[3], device_id=partner, device_id_type=MESH,
        )
    )
    for copy in small:
        copy.start()
    outward = [
        pltpu.make_async_copy(src, dst, local.at[k])
        for k, (src, dst) in enumerate(
            (
                (proj_own, all_proj.at[me]),
                (tables_own, all_tables.at[me]),
                (rates_own, all_rates.at[me]),
                (step_own, both_steps.at[core]),
            )
        )
    ]
    for copy in outward:
        copy.start()

    arrivals = (
        (left, 0, 0, to_right, 4),
        (right, 1, 2, to_left, 5),
        (left, 1, 1, None, None),
        (right, 0, 3, None, None),
        (across, 0, 4, None, None),
        (across, 1, 5, None, None),
    )
    for shard, quarter, slot, onward, onward_slot in arrivals:
        for k in (1, 0):
            piece(k, shard, quarter, k * 12 + slot, partner).wait_recv()
            if onward is not None:
                go(piece(k, shard, quarter, k * 12 + onward_slot, onward))
            go(piece(k, shard, quarter, k * 12 + 6 + slot, partner))

    def partner_rows(k, quarter):
        quarter_rows = pairs[k][0].shape[0] // 4
        return pl.ds(
            pl.multiple_of(((1 - core) * 2 + quarter) * quarter_rows, quarter_rows), quarter_rows
        )

    for shard, quarter, slot, _, _ in arrivals:
        for k in (1, 0):
            dst = pairs[k][1].at[shard, partner_rows(k, quarter)]
            remote(dst, dst, k * 12 + 6 + slot, partner).wait_recv()
    for copy in small:
        copy.wait_recv()
    for copy in started + small:
        copy.wait_send()
    for copy in outward:
        copy.wait()


def gather_over_tp(proj, tables, rates, step):
    count = lax.axis_size("tp")
    spec = pl.BlockSpec(memory_space=pl.ANY)
    return pl.pallas_call(
        gather_kernel,
        out_shape=(
            jax.ShapeDtypeStruct((count, *proj.shape), proj.dtype),
            jax.ShapeDtypeStruct((count, *tables.shape), tables.dtype),
            jax.ShapeDtypeStruct((count, *rates.shape), rates.dtype),
            jax.ShapeDtypeStruct((2, *step.shape), step.dtype),
        ),
        in_specs=[spec] * 4,
        out_specs=(spec,) * 4,
        scratch_shapes=[
            pltpu.VMEM(proj.shape, proj.dtype),
            pltpu.VMEM(tables.shape, tables.dtype),
            pltpu.VMEM(rates.shape, rates.dtype),
            pltpu.VMEM(step.shape, step.dtype),
            pltpu.SemaphoreType.DMA((24,)),
            pltpu.SemaphoreType.DMA((24,)),
            pltpu.SemaphoreType.DMA((4,)),
            pltpu.SemaphoreType.DMA((4,)),
            pltpu.SemaphoreType.DMA((4,)),
        ],
        compiler_params=pltpu.CompilerParams(
            collective_id=0, has_side_effects=True, vmem_limit_bytes=4 << 20
        ),
        name="gather_over_tp",
    )(proj, tables, rates, step)


def mixer_kernel(
    tokens, proj, tables, rates, steps, in_gain, out_gain, shaped,
    tok, wide, normed, drive, e_re, e_im, g_re, g_im, inj, pushed, total, answer, tau,
    send1, got1, carry_in, decays, plane_end, plane_got, plane_time, time_got, send3, got3,
    load, s1, r1, s2, r2, st, rt, s3, r3,
):
    rows = tok.shape[0]
    tp_count, sp_count = lax.axis_size("tp"), lax.axis_size("sp")
    planes = sp_count // 2
    members = 2 * tp_count
    me, sp = lax.axis_index("tp"), lax.axis_index("sp")
    core, plane = lax.rem(sp, 2), sp // 2
    place = core * tp_count + me
    tiles = e_re.shape[0]
    per_shard = tiles // tp_count
    shards = tp_count

    def member(k):
        return {"sp": plane * 2 + k // tp_count, "tp": k % tp_count}

    def at_plane(z):
        return {"sp": z * 2 + core}

    barrier = pltpu.get_barrier_semaphore()

    def greet(offset, carry):
        other = lax.rem(plane + offset, planes)
        pl.semaphore_signal(barrier, inc=1, device_id=at_plane(other), device_id_type=MESH)
        return carry

    lax.fori_loop(1, planes, greet, 0)
    for k in range(members):
        @pl.when(place != k)
        def _():
            pl.semaphore_signal(barrier, inc=1, device_id=member(k), device_id_type=MESH)

    loads = [
        pltpu.make_async_copy(tokens, tok, load.at[0]),
        pltpu.make_async_copy(proj, wide, load.at[1]),
    ]
    for copy in loads:
        copy.start()

    row = lax.broadcasted_iota(jnp.int32, (rows, LANES), 0)
    lane = lax.broadcasted_iota(jnp.int32, (rows, LANES), 1)
    step_rows = rows // LANES
    column = jnp.zeros((rows, 1), F32)
    for k in range(step_rows):
        line = steps[core, pl.ds(me * step_rows + k, 1), :]
        column += jnp.sum(
            jnp.where(lane + k * LANES <= row, jnp.broadcast_to(line, (rows, LANES)), 0.0),
            axis=1, keepdims=True,
        )
    tau[...] = jnp.broadcast_to(column, (rows, LANES))
    whole_plane = jnp.sum(jnp.sum(steps[0] + steps[1], axis=1, keepdims=True), axis=0, keepdims=True)
    plane_time[...] = jnp.broadcast_to(whole_plane, plane_time.shape)

    first_row = lax.broadcasted_iota(jnp.int32, (CHUNK, LANES), 0) == 0

    def tables_of(i, carry):
        shard, inner = i // per_shard, lax.rem(i, per_shard)
        rate = rates[shard, pl.ds(inner, 1), :]
        high, low = turns_of(rates[shard, pl.ds(per_shard + inner, 1), :])
        before_re = jnp.ones((CHUNK, LANES), F32)
        before_im = jnp.zeros((CHUNK, LANES), F32)
        for c in range(0, rows, CHUNK):
            here = pl.ds(c, CHUNK)
            times = tau[here, :]
            cosine, sine = rotation(high, low, times)
            exponent = rate * times
            shrink, grow = jnp.exp(-exponent), jnp.exp(exponent)
            e_re[i, here, :] = shrink * cosine
            e_im[i, here, :] = shrink * sine
            q_re, q_im = grow * cosine, -(grow * sine)
            turned_re, turned_im = pltpu.roll(q_re, 1, 0), pltpu.roll(q_im, 1, 0)
            g_re[i, here, :] = jnp.where(first_row, before_re, turned_re) - q_re
            g_im[i, here, :] = jnp.where(first_row, before_im, turned_im) - q_im
            before_re, before_im = turned_re, turned_im
        return carry

    lax.fori_loop(0, tiles, tables_of, 0)

    loads[0].wait()
    strip = 16

    def norm(i, carry):
        here = pl.ds(pl.multiple_of(i * strip, strip), strip)
        value = tok[here, :].astype(F32)
        scale = lax.rsqrt(jnp.mean(value * value, axis=1, keepdims=True) + 1e-06)
        normed[here, :] = (value * scale * in_gain[...]).astype(BF16)
        return carry

    lax.fori_loop(0, rows // strip, norm, 0)
    loads[1].wait()
    for t in range(0, shards, 2):
        both = jnp.dot(
            normed[...],
            jnp.concatenate([wide[t], wide[t + 1]], axis=1),
            preferred_element_type=F32,
        )
        drive[t] = both[:, :LANES].astype(BF16)
        drive[t + 1] = both[:, LANES:].astype(BF16)

    k_row = lax.broadcasted_iota(jnp.int32, (LANES, LANES), 0)
    k_lane = lax.broadcasted_iota(jnp.int32, (LANES, LANES), 1)
    group_rows = LANES // (2 * per_shard)

    def inject(i, half):
        shard, inner = i // per_shard, lax.rem(i, per_shard)
        mask = k_row // group_rows == 2 * inner + k_lane // CHUNK
        push = [
            jnp.where(mask, tables[shard, b * LANES : (b + 1) * LANES, :].astype(F32), 0.0).astype(BF16)
            for b in range(2)
        ]
        pushed[...] = jnp.dot(
            drive[shard], jnp.concatenate(push, axis=1), preferred_element_type=F32
        )
        sum_re = jnp.zeros((CHUNK, LANES), F32)
        sum_im = jnp.zeros((CHUNK, LANES), F32)
        for c in range(0, rows, CHUNK):
            here = pl.ds(c, CHUNK)
            u_re, u_im = pushed[here, :LANES], pushed[here, LANES:]
            a_re, a_im = g_re[i, here, :], g_im[i, here, :]
            w_re = a_re * u_re - a_im * u_im
            w_im = a_re * u_im + a_im * u_re
            sum_re += w_re
            sum_im += w_im
            inj[i, here, :LANES] = w_re.astype(BF16)
            inj[i, here, LANES:] = w_im.astype(BF16)
        t_re = jnp.sum(sum_re, axis=0, keepdims=True)
        t_im = jnp.sum(sum_im, axis=0, keepdims=True)
        d_re, d_im = e_re[i, rows - 1 : rows, :], e_im[i, rows - 1 : rows, :]
        part = i // 2
        send1[part, half : half + 1, :] = d_re * t_re - d_im * t_im
        send1[part, 2 + half : 3 + half, :] = d_re * t_im + d_im * t_re
        send1[part, 4 + half : 5 + half, :] = d_re
        send1[part, 6 + half : 7 + half, :] = d_im

    def inject_pair(part, carry):
        inject(2 * part, 0)
        inject(2 * part + 1, 1)
        return carry

    lax.fori_loop(0, tiles // 2, inject_pair, 0)

    pl.semaphore_wait(barrier, planes - 1 + members - 1)

    def copy1(k):
        return pltpu.make_async_remote_copy(
            src_ref=send1.at[k], dst_ref=got1.at[place], send_sem=s1.at[k], recv_sem=r1.at[place],
            device_id=member(k), device_id_type=MESH,
        )

    for k in range(members):
        @pl.when(place != k)
        def _():
            copy1(k).start()

    def copy_time(z):
        return pltpu.make_async_remote_copy(
            src_ref=plane_time, dst_ref=time_got.at[plane], send_sem=st.at[z],
            recv_sem=rt.at[plane], device_id=at_plane(z), device_id_type=MESH,
        )

    def loop(lower, upper, body):
        def step(z, carry):
            body(z)
            return carry

        lax.fori_loop(lower, upper, step, 0)

    loop(plane + 1, planes, lambda z: copy_time(z).start())
    got1[pl.ds(place, 1)] = send1[pl.ds(place, 1)]
    for k in range(members):
        @pl.when(place != k)
        def _():
            pltpu.make_async_remote_copy(
                src_ref=send1.at[k], dst_ref=got1.at[k], send_sem=s1.at[k], recv_sem=r1.at[k],
                device_id=member(k), device_id_type=MESH,
            ).wait_recv()

    def advance(k, re, im):
        block = got1[k]
        d_re, d_im = block[4:6], block[6:8]
        return d_re * re - d_im * im + block[0:2], d_re * im + d_im * re + block[2:4]

    nothing = jnp.zeros((2, LANES), F32)
    re, im = nothing, nothing
    for k in range(members):
        re, im = advance(k, re, im)
    plane_end[0:2, :] = re
    plane_end[2:4, :] = im

    def copy2(z):
        return pltpu.make_async_remote_copy(
            src_ref=plane_end, dst_ref=plane_got.at[plane], send_sem=s2.at[z],
            recv_sem=r2.at[plane], device_id=at_plane(z), device_id_type=MESH,
        )

    loop(plane + 1, planes, lambda z: copy2(z).start())

    p_row = lax.broadcasted_iota(jnp.int32, (rows, rows), 0)
    p_col = lax.broadcasted_iota(jnp.int32, (rows, rows), 1)
    lower = jnp.where(p_col <= p_row, 1.0, 0.0).astype(BF16)

    def prefix(i):
        total[i] = jnp.dot(lower, inj[i], preferred_element_type=F32)

    loop(0, tiles, prefix)

    def time_wait(z):
        pltpu.make_async_remote_copy(
            src_ref=plane_time, dst_ref=time_got.at[z], send_sem=st.at[z], recv_sem=rt.at[z],
            device_id=at_plane(z), device_id_type=MESH,
        ).wait_recv()

    loop(0, plane, time_wait)

    def plane_decay(z):
        times = jnp.broadcast_to(time_got[z], (1, LANES))
        for half in range(2):
            i = 2 * place + half
            shard, inner = i // per_shard, lax.rem(i, per_shard)
            rate = rates[shard, pl.ds(inner, 1), :]
            high, low = turns_of(rates[shard, pl.ds(per_shard + inner, 1), :])
            cosine, sine = rotation(high, low, times)
            shrink = jnp.exp(-(rate * times))
            decays[z, half : half + 1, :] = shrink * cosine
            decays[z, 2 + half : 3 + half, :] = shrink * sine

    loop(0, plane, plane_decay)

    def end_wait(z):
        pltpu.make_async_remote_copy(
            src_ref=plane_end, dst_ref=plane_got.at[z], send_sem=s2.at[z], recv_sem=r2.at[z],
            device_id=at_plane(z), device_id_type=MESH,
        ).wait_recv()

    loop(0, plane, end_wait)

    def earlier(z, carry):
        re, im = carry
        d, end = decays[z], plane_got[z]
        return (
            d[0:2] * re - d[2:4] * im + end[0:2],
            d[0:2] * im + d[2:4] * re + end[2:4],
        )

    re, im = lax.fori_loop(0, plane, earlier, (nothing, nothing))
    for k in range(members):
        send3[k, 0:2, :] = re
        send3[k, 2:4, :] = im
        if k < members - 1:
            re, im = advance(k, re, im)

    def copy3(k):
        return pltpu.make_async_remote_copy(
            src_ref=send3.at[k], dst_ref=got3.at[place], send_sem=s3.at[k], recv_sem=r3.at[place],
            device_id=member(k), device_id_type=MESH,
        )

    for k in range(members):
        @pl.when(place != k)
        def _():
            copy3(k).start()
    got3[pl.ds(place, 1)] = send3[pl.ds(place, 1)]
    for k in range(members):
        @pl.when(place != k)
        def _():
            pltpu.make_async_remote_copy(
                src_ref=send3.at[k], dst_ref=got3.at[k], send_sem=s3.at[k], recv_sem=r3.at[k],
                device_id=member(k), device_id_type=MESH,
            ).wait_recv()

    answer[...] = jnp.zeros_like(answer)

    def respond(i, half):
        shard, inner = i // per_shard, lax.rem(i, per_shard)
        part = i // 2
        in_re = got3[part, half : half + 1, :]
        in_im = got3[part, 2 + half : 3 + half, :]
        for c in range(0, rows, CHUNK):
            here = pl.ds(c, CHUNK)
            a_re, a_im = total[i, here, :LANES] + in_re, total[i, here, LANES:] + in_im
            p_re, p_im = e_re[i, here, :], e_im[i, here, :]
            inj[i, here, :LANES] = (p_re * a_re - p_im * a_im).astype(BF16)
            inj[i, here, LANES:] = (p_re * a_im + p_im * a_re).astype(BF16)
        read = tables[shard, 2 * LANES :, :].astype(F32)
        lane_group = lax.broadcasted_iota(jnp.int32, (CHUNK, LANES), 1) // group_rows
        blocks = [
            jnp.where(lane_group == 2 * inner + g, read[b * CHUNK : (b + 1) * CHUNK], 0.0)
            for b in range(2)
            for g in range(2)
        ]
        answer[shard] += jnp.dot(
            inj[i], jnp.concatenate(blocks, axis=0).astype(BF16), preferred_element_type=F32
        )

    def respond_pair(part):
        respond(2 * part, 0)
        respond(2 * part + 1, 1)

    loop(0, tiles // 2, respond_pair)

    def finish(i):
        here = pl.ds(pl.multiple_of(i * CHUNK, CHUNK), CHUNK)
        values = []
        squares = jnp.zeros((CHUNK, LANES), F32)
        for t in range(shards):
            v = answer[t, here, :]
            v = 0.5 * v * (1.0 + jnp.tanh(0.7978845608 * (v + 0.044715 * (v * v * v))))
            v = v.astype(BF16).astype(F32)
            values.append(v)
            squares += v * v
        mean = jnp.sum(squares, axis=1, keepdims=True) * np.float32(1.0 / (shards * LANES))
        scale = lax.rsqrt(mean + 1e-06)
        for t in range(shards):
            line = pl.ds(t * LANES, LANES)
            shaped[here, line] = (values[t] * scale * out_gain[:, line]).astype(BF16)

    loop(0, rows // CHUNK, finish)

    for k in range(members):
        @pl.when(place != k)
        def _():
            copy1(k).wait_send()
            copy3(k).wait_send()
    loop(plane + 1, planes, lambda z: copy_time(z).wait_send())
    loop(plane + 1, planes, lambda z: copy2(z).wait_send())


def mix(tokens, proj, tables, rates, steps, in_gain, out_gain):
    rows, width = tokens.shape
    shards = lax.axis_size("tp")
    planes = lax.axis_size("sp") // 2
    members = 2 * shards
    tiles = shards * rates.shape[1] // 2
    vmem = pl.BlockSpec(memory_space=pltpu.VMEM)
    far = pl.BlockSpec(memory_space=pl.ANY)
    table = pltpu.VMEM((tiles, rows, LANES), F32)
    dma = pltpu.SemaphoreType.DMA
    return pl.pallas_call(
        mixer_kernel,
        out_shape=jax.ShapeDtypeStruct((rows, shards * LANES), BF16),
        in_specs=[far, far] + [vmem] * 5,
        out_specs=vmem,
        scratch_shapes=[
            pltpu.VMEM(tokens.shape, BF16),
            pltpu.VMEM(proj.shape, BF16),
            pltpu.VMEM(tokens.shape, BF16),
            pltpu.VMEM((shards, rows, LANES), BF16),
            table, table, table, table,
            pltpu.VMEM((tiles, rows, 2 * LANES), BF16),
            pltpu.VMEM((rows, 2 * LANES), F32),
            pltpu.VMEM((tiles, rows, 2 * LANES), F32),
            pltpu.VMEM((shards, rows, LANES), F32),
            pltpu.VMEM((rows, LANES), F32),
            pltpu.VMEM((members, 8, LANES), F32),
            pltpu.VMEM((members, 8, LANES), F32),
            pltpu.VMEM((4, LANES), F32),
            pltpu.VMEM((planes, 4, LANES), F32),
            pltpu.VMEM((4, LANES), F32),
            pltpu.VMEM((planes, 4, LANES), F32),
            pltpu.VMEM((1, LANES), F32),
            pltpu.VMEM((planes, 1, LANES), F32),
            pltpu.VMEM((members, 4, LANES), F32),
            pltpu.VMEM((members, 4, LANES), F32),
            dma((2,)),
            dma((members,)), dma((members,)),
            dma((planes,)), dma((planes,)),
            dma((planes,)), dma((planes,)),
            dma((members,)), dma((members,)),
        ],
        compiler_params=pltpu.CompilerParams(
            collective_id=1, has_side_effects=True, vmem_limit_bytes=48 << 20
        ),
        name="mixer",
    )(tokens, proj, tables, rates, steps, in_gain, out_gain)


def on_device(
    tokens, step, in_gain, in_proj, decay_rate, frequency, input_map, readout, out_gain, out_proj
):
    groups, states = decay_rate.shape
    lam_re, lam_im = -decay_rate[:, :, None], frequency[:, :, None]
    size = lam_re * lam_re + lam_im * lam_im
    b_re = (input_map[0] * lam_re + input_map[1] * lam_im) / size
    b_im = (input_map[1] * lam_re - input_map[0] * lam_im) / size
    rows = groups * input_map.shape[-1]
    push = jnp.stack([b_re, b_re, b_im, b_im]).transpose(1, 3, 0, 2).reshape(rows, 2, 2 * states)
    push = push.transpose(1, 0, 2).reshape(2 * rows, 2 * states)
    read = jnp.stack([readout[0], -readout[1]]).transpose(0, 3, 1, 2).reshape(2 * states, rows)
    tables = jnp.concatenate([push, read], axis=0).astype(BF16)
    rates = jnp.concatenate([decay_rate, frequency], axis=0).reshape(-1, LANES)
    proj, tables, rates, steps = gather_over_tp(in_proj, tables, rates, step.reshape(-1, LANES))
    shaped = mix(
        tokens, proj, tables, rates, steps, in_gain.reshape(1, -1), out_gain.reshape(1, -1)
    )
    return jnp.dot(shaped, out_proj, preferred_element_type=F32).astype(BF16)


def solution(mesh):
    placed = (
        P(("grp", "sp", "tp"), None),
        P(("grp", "sp")),
        P(),
        P(None, "tp"),
        P("tp", None),
        P("tp", None),
        P(None, "tp", None, None),
        P(None, "tp", None, None),
        P(),
        P(),
    )
    return jax.shard_map(
        on_device,
        mesh=mesh,
        in_specs=placed,
        out_specs=P(("grp", "sp", "tp"), None),
        check_vma=False,
    )
```

time: 378 us -> 90.6 us (0.24); the launches traced: 373 us -> 90.3 us
  matrix products: 134 us -> 1.69 us
  waiting for transfers between devices: 85.1 us -> 0 us
  Pallas kernels: 0 us -> 81.9 us
  blocking collectives: 69.5 us -> 0 us
  local copies, waits for them, and re-layouts: 43.1 us -> 3.16 us
  other arithmetic: 22.5 us -> 3.43 us
  between operations: 13.7 us -> 0.13 us
  loops' own time: 5.22 us -> 0 us
    dot_general x84 -> x1, matrix products: 134 us -> 1.69 us  [on_device(): return jnp.dot(shaped, out_proj, preferred_element_type=F32).astype(BF16)]
    all_gather x1 -> x0, waiting for transfers between devices: 85.1 us -> none  [on_device(): lax.all_gather(normed, 'tp', axis=0, tiled=True)]
    pallas_call x0 -> x2, Pallas kernels: none -> 81.9 us  [the longest x1 54.3 us: gather_over_tp(): pl.pallas_call(gather_kernel, out_shape=(jax.ShapeDtypeStruct((count, *pr...]
    all_gather x1 -> x0, blocking collectives: 60.4 us -> none  [gathered_once(): both, at, found = (lax.all_gather(jnp.concatenate(lines), axis), 0, {})]
    slice x33 -> x1, local copies, waits for them, and re-layouts: 19.1 us -> 0.84 us  [on_device(): readout[0]]
    squeeze x20 -> x0, local copies, waits for them, and re-layouts: 11.6 us -> none  [the longest x16 11.6 us: on_device(): lax.scan(partial(advance, rates=flat_rates, freqs=flat_freqs, tables=tabl...]
    all_to_all x1 -> x0, blocking collectives: 9.19 us -> none  [on_device(): lax.all_to_all(answer, 'tp', split_axis=0, concat_axis=1, tiled=True)]
    mul x16 -> x0, other arithmetic: 8.87 us -> none  [advance(): c_re = shrink * cosine]
  transfers between devices with their start and end apart: 1 -> 0, of which waited for: 1 -> 0; matrix products, arithmetic and copies ran while one was open for 1% -> 0% of each run, Pallas kernels for 0% -> 0%
where the time goes in v1:
time: 90.6 us; the launch traced here: 90.3 us
  Pallas kernels  81.9 us (90%)
  other arithmetic  3.43 us (4%)
  local copies, waits for them, and re-layouts  3.16 us (3%)
  matrix products  1.69 us (2%)
    pallas_call x1, Pallas kernels, gather_over_tp(): pl.pallas_call(gather_kernel, out_shape=(jax.ShapeDtypeStruct((count, *pr...  54.3 us
    pallas_call x1, Pallas kernels, mix(): pl.pallas_call(mixer_kernel, out_shape=jax.ShapeDtypeStruct((rows, shards...  27.6 us

profile of v1, /device:TPU:33, one launch (start us, length us, event | category | flops | bytes accessed | tf_op | source)
XLA Modules:
  0.0 90.3 jit_solution(9507045466132891244)
XLA Ops:
  0.0 0.0 copy-start
  0.0 0.0 copy-start.5
  0.0 0.0 copy-start.3
  0.0 0.0 copy-start.1
  0.0 0.9 pad_maximum_fusion.1
  0.9 0.1 reshape.34.rates
  1.0 0.8 fusion
  1.7 0.8 negate_convert_fusion
  2.6 0.8 slice.26
  3.4 0.1 copy.14
  3.5 0.1 reshape.33
  3.6 0.1 copy.15
  3.7 0.9 %divide_convert_fusion.1 = (bf16[1,8,64,16]{2,3,1,0:T(8,128)(2,1)S(1)}, bf16[1,8,64,16]{2,3,1,0:T(8,128)(2,1)S(1)}) fusion(f32[2,8,64,16]{2,3,1,0:T(8,128)} %param.16, f32[8,64]{1,0:T(8,128)S(1)} %get-tuple-element.16, f32[8,64]{1,0:T(8,128)} %param.15, f32[8,64]{1,0:T(8,128)S(1)} %get-tuple-element.15), kind=kLoop, calls=%fused_computation.7 | loop fusion | flops 81920 | bytes 104448 | tf_op jit(solution)/shard_map/convert.11
  4.7 0.1 copy.12
  4.8 0.1 reshape.31
  4.9 0.0 copy-start.2
  4.9 1.0 %copy-done.2 = bf16[2048,128]{1,0:T(8,128)(2,1)S(1)} copy-done((bf16[2048,128]{1,0:T(8,128)(2,1)S(1)}, bf16[2048,128]{1,0:T(8,128)(2,1)}, u32[]{:S(2)}) %copy-start.2) | copy-done | bytes 524312
  6.0 0.0 copy-start.4
  6.0 0.7 copy-done.4
  6.7 54.3 %gather_over_tp.1 = (bf16[4,2048,128]{2,1,0:T(8,128)(2,1)S(1)}, bf16[4,384,128]{2,1,0:T(8,128)(2,1)S(1)}, f32[4,8,128]{2,1,0:T(8,128)S(1)}, f32[2,8,128]{2,1,0:T(8,128)S(1)}) custom-call(bf16[2048,128]{1,0:T(8,128)(2,1)S(1)} %copy-done.2, bf16[384,128]{1,0:T(8,128)(2,1)S(1)} %pad_maximum_fusion.tables, f32[8,128]{1,0:T(8,128)S(1)} %reshape.34.rates, ...), custom_call_target="tpu_custom_call" | custom-call | tf_op jit(solution)/shard_map/gather_over_tp/pallas_call | solution.py:171
  60.9 0.0 copy-done.5
  61.0 0.0 copy-done.3
  61.0 0.0 copy-done.1
  61.0 27.6 %mixer.1 = bf16[256,512]{1,0:T(8,128)(2,1)S(1)} custom-call(bf16[256,2048]{1,0:T(8,128)(2,1)S(1)} %copy-done.1, bf16[4,2048,128]{2,1,0:T(8,128)(2,1)S(1)} %get-tuple-element.9.proj, bf16[4,384,128]{2,1,0:T(8,128)(2,1)S(1)} %get-tuple-element.10.tables, f32[4,8,128]{2,1,0:T(8,128)S(1)} %get-tuple-element.11.rates, f32[2,8,128]{2,1,0:T(8,128)S(1)} %get-tuple-element.12.steps, ...), custom_call_target="tpu_custom_call" | custom-call | tf_op jit(solution)/shard_map/mixer/pallas_call | solution.py:540
  88.6 0.0 copy-done
  88.6 1.7 %convolution_convert_fusion = bf16[256,2048]{1,0:T(8,128)(2,1)} fusion(bf16[256,512]{1,0:T(8,128)(2,1)S(1)} %mixer.1, bf16[512,2048]{1,0:T(8,128)(2,1)S(1)} %copy-done), kind=kOutput, calls=%fused_computation | convolution fusion | flops 537395200 | bytes 3407872 | tf_op jit(solution)/shard_map/dot_general | solution.py:597
  (4 shorter events, 0.1 us)
Async XLA Ops:
  0.0 88.6 %copy-start = (bf16[512,2048]{1,0:T(8,128)(2,1)S(1)}, bf16[512,2048]{1,0:T(8,128)(2,1)}, u32[]{:S(2)}) copy-start(bf16[512,2048]{1,0:T(8,128)(2,1)} %param.19) | copy-start | bytes 6291460
  0.0 60.9 %copy-start.5 = (f32[512]{0:T(512)S(1)}, f32[512]{0:T(512)}, u32[]{:S(2)}) copy-start(f32[512]{0:T(512)} %param.18) | copy-start | bytes 6148
  0.0 61.0 %copy-start.3 = (f32[2048]{0:T(1024)S(1)}, f32[2048]{0:T(1024)}, u32[]{:S(2)}) copy-start(f32[2048]{0:T(1024)} %param.12) | copy-start | bytes 24580
  0.0 61.0 %copy-start.1 = (bf16[256,2048]{1,0:T(8,128)(2,1)S(1)}, bf16[256,2048]{1,0:T(8,128)(2,1)}, u32[]{:S(2)}) copy-start(bf16[256,2048]{1,0:T(8,128)(2,1)} %tokens.1) | copy-start | bytes 3145732
  4.9 1.0 %copy-start.2 = (bf16[2048,128]{1,0:T(8,128)(2,1)S(1)}, bf16[2048,128]{1,0:T(8,128)(2,1)}, u32[]{:S(2)}) copy-start(bf16[2048,128]{1,0:T(8,128)(2,1)} %proj.1) | copy-start | bytes 1572868
  6.0 0.7 copy-start.4

commit v2 on v1

--- a/solution.py
+++ b/solution.py
@@ -46,51 +46,18 @@
     return polynomial(square, COS), polynomial(square, SIN) * part
 
 
-def gather_kernel(
-    proj, tables, rates, step, all_proj, all_tables, all_rates, both_steps,
-    proj_own, tables_own, rates_own, step_own, send, recv, small_send, small_recv, local,
-):
-    count = lax.axis_size("tp")
-    me, sp = lax.axis_index("tp"), lax.axis_index("sp")
-    core = lax.rem(sp, 2)
-    partner = {"sp": sp + 1 - 2 * core}
-    right, left = lax.rem(me + 1, count), lax.rem(me + count - 1, count)
-    across = lax.rem(me + 2, count)
-    to_right, to_left, to_across = {"tp": right}, {"tp": left}, {"tp": across}
-
-    barrier = pltpu.get_barrier_semaphore()
-    for target in (to_right, to_left, to_across, partner):
-        pl.semaphore_signal(barrier, inc=1, device_id=target, device_id_type=MESH)
-
-    inward = [
-        pltpu.make_async_copy(src, dst, local.at[k])
-        for k, (src, dst) in enumerate(
-            ((proj, proj_own), (tables, tables_own), (rates, rates_own), (step, step_own))
-        )
-    ]
-    for copy in inward:
-        copy.start()
-    for copy in inward:
-        copy.wait()
-    pl.semaphore_wait(barrier, 4)
-
-    pairs = ((proj_own, all_proj), (tables_own, all_tables))
-
-    def rows(k, quarter):
-        quarter_rows = pairs[k][0].shape[0] // 4
-        return pl.ds(pl.multiple_of((core * 2 + quarter) * quarter_rows, quarter_rows), quarter_rows)
-
-    def remote(src, dst, slot, target):
+def gather_over_tp(wide, tables, rates, proj_sent, proj_got, table_sent, table_got, rate_sent, rate_got):
+    count, me = lax.axis_size("tp"), lax.axis_index("tp")
+    right, left, across = (lax.rem(me + k, count) for k in (1, count - 1, 2))
+
+    def piece(k, shard, half, slot, target):
+        ref, sent, got = ((wide, proj_sent, proj_got), (tables, table_sent, table_got))[k]
+        size = ref.shape[1] // 2
+        where = ref.at[shard, pl.ds(half * size, size)]
         return pltpu.make_async_remote_copy(
-            src_ref=src, dst_ref=dst, send_sem=send.at[slot], recv_sem=recv.at[slot],
-            device_id=target, device_id_type=MESH,
-        )
-
-    def piece(k, shard, quarter, slot, target, own=False):
-        own_ref, all_ref = pairs[k]
-        where = rows(k, quarter)
-        dst = all_ref.at[shard, where]
-        return remote(own_ref.at[where] if own else dst, dst, slot, target)
+            src_ref=where, dst_ref=where, send_sem=sent.at[slot], recv_sem=got.at[slot],
+            device_id={"tp": target}, device_id_type=MESH,
+        )
 
     started = []
 
@@ -98,109 +65,82 @@
         copy.start()
         started.append(copy)
 
+    small = [
+        pltpu.make_async_remote_copy(
+            src_ref=rates.at[me], dst_ref=rates.at[me], send_sem=rate_sent.at[slot],
+            recv_sem=rate_got.at[slot], device_id={"tp": target}, device_id_type=MESH,
+        )
+        for slot, target in enumerate((right, left, across))
+    ]
+    for copy in small:
+        go(copy)
     for order in range(2):
         for k in (1, 0):
-            go(piece(k, me, order, k * 12 + order, to_right, own=True))
-            go(piece(k, me, 1 - order, k * 12 + 2 + order, to_left, own=True))
-    small = []
-    for slot, target in enumerate((to_right, to_left, to_across)):
-        small.append(
-            pltpu.make_async_remote_copy(
-                src_ref=rates_own, dst_ref=all_rates.at[me], send_sem=small_send.at[slot],
-                recv_sem=small_recv.at[slot], device_id=target, device_id_type=MESH,
-            )
-        )
-    small.append(
-        pltpu.make_async_remote_copy(
-            src_ref=step_own, dst_ref=both_steps.at[core], send_sem=small_send.at[3],
-            recv_sem=small_recv.at[3], device_id=partner, device_id_type=MESH,
-        )
-    )
-    for copy in small:
-        copy.start()
-    outward = [
-        pltpu.make_async_copy(src, dst, local.at[k])
-        for k, (src, dst) in enumerate(
-            (
-                (proj_own, all_proj.at[me]),
-                (tables_own, all_tables.at[me]),
-                (rates_own, all_rates.at[me]),
-                (step_own, both_steps.at[core]),
-            )
-        )
-    ]
-    for copy in outward:
-        copy.start()
-
-    arrivals = (
-        (left, 0, 0, to_right, 4),
-        (right, 1, 2, to_left, 5),
+            go(piece(k, me, order, order, right))
+            go(piece(k, me, 1 - order, 2 + order, left))
+    for shard, half, slot, onward, onward_slot in (
+        (left, 0, 0, right, 4),
+        (right, 1, 2, left, 5),
         (left, 1, 1, None, None),
         (right, 0, 3, None, None),
         (across, 0, 4, None, None),
         (across, 1, 5, None, None),
-    )
-    for shard, quarter, slot, onward, onward_slot in arrivals:
+    ):
         for k in (1, 0):
-            piece(k, shard, quarter, k * 12 + slot, partner).wait_recv()
+            piece(k, shard, half, slot, left).wait_recv()
             if onward is not None:
-                go(piece(k, shard, quarter, k * 12 + onward_slot, onward))
-            go(piece(k, shard, quarter, k * 12 + 6 + slot, partner))
-
-    def partner_rows(k, quarter):
-        quarter_rows = pairs[k][0].shape[0] // 4
-        return pl.ds(
-            pl.multiple_of(((1 - core) * 2 + quarter) * quarter_rows, quarter_rows), quarter_rows
-        )
-
-    for shard, quarter, slot, _, _ in arrivals:
-        for k in (1, 0):
-            dst = pairs[k][1].at[shard, partner_rows(k, quarter)]
-            remote(dst, dst, k * 12 + 6 + slot, partner).wait_recv()
+                go(piece(k, shard, half, onward_slot, onward))
     for copy in small:
         copy.wait_recv()
-    for copy in started + small:
+    for copy in started:
         copy.wait_send()
-    for copy in outward:
-        copy.wait()
-
-
-def gather_over_tp(proj, tables, rates, step):
-    count = lax.axis_size("tp")
-    spec = pl.BlockSpec(memory_space=pl.ANY)
-    return pl.pallas_call(
-        gather_kernel,
-        out_shape=(
-            jax.ShapeDtypeStruct((count, *proj.shape), proj.dtype),
-            jax.ShapeDtypeStruct((count, *tables.shape), tables.dtype),
-            jax.ShapeDtypeStruct((count, *rates.shape), rates.dtype),
-            jax.ShapeDtypeStruct((2, *step.shape), step.dtype),
-        ),
-        in_specs=[spec] * 4,
-        out_specs=(spec,) * 4,
-        scratch_shapes=[
-            pltpu.VMEM(proj.shape, proj.dtype),
-            pltpu.VMEM(tables.shape, tables.dtype),
-            pltpu.VMEM(rates.shape, rates.dtype),
-            pltpu.VMEM(step.shape, step.dtype),
-            pltpu.SemaphoreType.DMA((24,)),
-            pltpu.SemaphoreType.DMA((24,)),
-            pltpu.SemaphoreType.DMA((4,)),
-            pltpu.SemaphoreType.DMA((4,)),
-            pltpu.SemaphoreType.DMA((4,)),
-        ],
-        compiler_params=pltpu.CompilerParams(
-            collective_id=0, has_side_effects=True, vmem_limit_bytes=4 << 20
-        ),
-        name="gather_over_tp",
-    )(proj, tables, rates, step)
+
+
+def own_tables(tables, rates, me, decay, frequency, input_map, readout):
+    groups, states = decay.shape
+    channels = input_map.shape[-1]
+    pairs = groups // 2
+    for g in range(groups):
+        lanes = slice((g % 2) * states, (g % 2 + 1) * states)
+        rates[me, g // 2 : g // 2 + 1, lanes] = decay[g : g + 1, :]
+        rates[me, pairs + g // 2 : pairs + g // 2 + 1, lanes] = frequency[g : g + 1, :]
+
+    def turned(value):
+        size = value.shape[1]
+        unit = jnp.where(
+            lax.broadcasted_iota(jnp.int32, (size, size), 0)
+            == lax.broadcasted_iota(jnp.int32, (size, size), 1),
+            1.0, 0.0,
+        ).astype(F32)
+        return lax.dot_general(
+            unit, value, (((1,), (1,)), ((), ())),
+            precision=lax.Precision.HIGHEST, preferred_element_type=F32,
+        )
+
+    maps = [turned(input_map[c].reshape(groups * states, channels)) for c in range(2)]
+    for k in range(pairs):
+        lam_re = -rates[me, k : k + 1, :]
+        lam_im = rates[me, pairs + k : pairs + k + 1, :]
+        size = lam_re * lam_re + lam_im * lam_im
+        m_re, m_im = (m[:, k * LANES : (k + 1) * LANES] for m in maps)
+        at = 2 * channels * k
+        tables[me, at : at + channels, :] = ((m_re * lam_re + m_im * lam_im) / size).astype(BF16)
+        tables[me, at + channels : at + 2 * channels, :] = (
+            (m_im * lam_re - m_re * lam_im) / size
+        ).astype(BF16)
+    for c, sign in ((0, 1.0), (1, -1.0)):
+        value = sign * turned(readout[c].reshape(groups * channels, states))
+        tables[me, LANES + c * states : LANES + (c + 1) * states, :] = value.astype(BF16)
 
 
 def mixer_kernel(
-    tokens, proj, tables, rates, steps, in_gain, out_gain, shaped,
-    tok, wide, normed, drive, e_re, e_im, g_re, g_im, inj, pushed, total, answer, tau,
-    send1, got1, carry_in, decays, plane_end, plane_got, plane_time, time_got, send3, got3,
+    tokens, proj, decay, frequency, input_map, readout, step, in_gain, out_gain, shaped,
+    tok, wide, tables, rates, steps, decay_in, frequency_in, input_map_in, readout_in,
+    normed, drive, e_re, e_im, g_re, g_im, inj, pushed, total, answer, tau,
+    send1, got1, decays, plane_end, plane_got, plane_time, time_got, send3, got3,
     load, s1, r1, s2, r2, st, rt, s3, r3,
+    proj_sent, proj_got, table_sent, table_got, rate_sent, rate_got, pass_sent, pass_got,
+    ready, all_in,
 ):
     rows = tok.shape[0]
     tp_count, sp_count = lax.axis_size("tp"), lax.axis_size("sp")
@@ -219,39 +159,128 @@
     def at_plane(z):
         return {"sp": z * 2 + core}
 
+    partner = {"sp": sp + 1 - 2 * core}
+    leads = place == 0
+
+    def loop(lower, upper, body):
+        def step(z, carry):
+            body(z)
+            return carry
+
+        lax.fori_loop(lower, upper, step, 0)
+
     barrier = pltpu.get_barrier_semaphore()
 
-    def greet(offset, carry):
-        other = lax.rem(plane + offset, planes)
-        pl.semaphore_signal(barrier, inc=1, device_id=at_plane(other), device_id_type=MESH)
-        return carry
-
-    lax.fori_loop(1, planes, greet, 0)
-    for k in range(members):
-        @pl.when(place != k)
-        def _():
-            pl.semaphore_signal(barrier, inc=1, device_id=member(k), device_id_type=MESH)
+    def greet(target):
+        pl.semaphore_signal(barrier, inc=1, device_id=target, device_id_type=MESH)
+
+    loop(0, plane, lambda z: greet({"sp": 2 * z}))
+
+    @pl.when(core == 1)
+    def _():
+        for k in range(1, tp_count):
+            greet({"tp": lax.rem(me + k, tp_count)})
+        greet(partner)
+
+    @pl.when(jnp.logical_and(jnp.logical_not(leads), place != tp_count))
+    def _():
+        greet({"sp": 2 * plane, "tp": 0})
 
     loads = [
         pltpu.make_async_copy(tokens, tok, load.at[0]),
-        pltpu.make_async_copy(proj, wide, load.at[1]),
+        pltpu.make_async_copy(proj, wide.at[me], load.at[1]),
     ]
     for copy in loads:
         copy.start()
+
+    passed = [
+        (rates, rates),
+        (tables, tables),
+        *((wide.at[lax.rem(me + k, tp_count)],) * 2 for k in range(1, tp_count)),
+        (step, steps.at[1]),
+    ]
+
+    def pass_on(slot):
+        src, dst = passed[slot]
+        return pltpu.make_async_remote_copy(
+            src_ref=src, dst_ref=dst, send_sem=pass_sent.at[slot], recv_sem=pass_got.at[slot],
+            device_id=partner, device_id_type=MESH,
+        )
+
+    def pass_back():
+        slot = len(passed)
+        return pltpu.make_async_remote_copy(
+            src_ref=step, dst_ref=steps.at[0], send_sem=pass_sent.at[slot],
+            recv_sem=pass_got.at[slot], device_id=partner, device_id_type=MESH,
+        )
+
+    @pl.when(core == 1)
+    def _():
+        inward = [
+            pltpu.make_async_copy(src, dst, load.at[2 + k])
+            for k, (src, dst) in enumerate(
+                (
+                    (decay, decay_in),
+                    (frequency, frequency_in),
+                    (input_map, input_map_in),
+                    (readout, readout_in),
+                )
+            )
+        ]
+        for copy in inward:
+            copy.start()
+        for copy in inward:
+            copy.wait()
+        own_tables(tables, rates, me, decay_in, frequency_in, input_map_in, readout_in)
+        loads[1].wait()
+        pl.semaphore_wait(barrier, tp_count - 1)
+        gather_over_tp(
+            wide, tables, rates, proj_sent, proj_got, table_sent, table_got, rate_sent, rate_got
+        )
+
+    later = 2 * (planes - 1 - plane)
+
+    @pl.when(leads)
+    def _():
+        pl.semaphore_wait(barrier, members - 1 + later)
+        pl.semaphore_signal(ready, inc=1, device_id=partner, device_id_type=MESH)
+        for k in range(1, members):
+            pl.semaphore_signal(all_in, inc=1, device_id=member(k), device_id_type=MESH)
+
+    @pl.when(jnp.logical_and(core == 0, jnp.logical_not(leads)))
+    def _():
+        pl.semaphore_wait(barrier, 1 + later)
+        pl.semaphore_signal(ready, inc=1, device_id=partner, device_id_type=MESH)
+
+    @pl.when(core == 0)
+    def _():
+        pass_back().start()
 
     row = lax.broadcasted_iota(jnp.int32, (rows, LANES), 0)
     lane = lax.broadcasted_iota(jnp.int32, (rows, LANES), 1)
     step_rows = rows // LANES
     column = jnp.zeros((rows, 1), F32)
     for k in range(step_rows):
-        line = steps[core, pl.ds(me * step_rows + k, 1), :]
+        line = step[pl.ds(me * step_rows + k, 1), :]
         column += jnp.sum(
             jnp.where(lane + k * LANES <= row, jnp.broadcast_to(line, (rows, LANES)), 0.0),
             axis=1, keepdims=True,
         )
     tau[...] = jnp.broadcast_to(column, (rows, LANES))
-    whole_plane = jnp.sum(jnp.sum(steps[0] + steps[1], axis=1, keepdims=True), axis=0, keepdims=True)
-    plane_time[...] = jnp.broadcast_to(whole_plane, plane_time.shape)
+    loads[0].wait()
+    strip = 16
+
+    def norm(i, carry):
+        here = pl.ds(pl.multiple_of(i * strip, strip), strip)
+        value = tok[here, :].astype(F32)
+        scale = lax.rsqrt(jnp.mean(value * value, axis=1, keepdims=True) + 1e-06)
+        normed[here, :] = (value * scale * in_gain[...]).astype(BF16)
+        return carry
+
+    lax.fori_loop(0, rows // strip, norm, 0)
+    @pl.when(core == 0)
+    def _():
+        pass_on(0).wait_recv()
 
     first_row = lax.broadcasted_iota(jnp.int32, (CHUNK, LANES), 0) == 0
 
@@ -278,18 +307,12 @@
 
     lax.fori_loop(0, tiles, tables_of, 0)
 
-    loads[0].wait()
-    strip = 16
-
-    def norm(i, carry):
-        here = pl.ds(pl.multiple_of(i * strip, strip), strip)
-        value = tok[here, :].astype(F32)
-        scale = lax.rsqrt(jnp.mean(value * value, axis=1, keepdims=True) + 1e-06)
-        normed[here, :] = (value * scale * in_gain[...]).astype(BF16)
-        return carry
-
-    lax.fori_loop(0, rows // strip, norm, 0)
-    loads[1].wait()
+    @pl.when(core == 0)
+    def _():
+        loads[1].wait()
+        for slot in range(1, len(passed)):
+            pass_on(slot).wait_recv()
+
     for t in range(0, shards, 2):
         both = jnp.dot(
             normed[...],
@@ -307,7 +330,21 @@
         shard, inner = i // per_shard, lax.rem(i, per_shard)
         mask = k_row // group_rows == 2 * inner + k_lane // CHUNK
         push = [
-            jnp.where(mask, tables[shard, b * LANES : (b + 1) * LANES, :].astype(F32), 0.0).astype(BF16)
+            jnp.where(
+                mask,
+                jnp.concatenate(
+                    [
+                        tables[
+                            shard,
+                            pl.ds(pl.multiple_of((2 * inner + b) * group_rows, group_rows), group_rows),
+                            :,
+                        ].astype(F32)
+                    ]
+                    * (LANES // group_rows),
+                    axis=0,
+                ),
+                0.0,
+            ).astype(BF16)
             for b in range(2)
         ]
         pushed[...] = jnp.dot(
@@ -341,7 +378,15 @@
 
     lax.fori_loop(0, tiles // 2, inject_pair, 0)
 
-    pl.semaphore_wait(barrier, planes - 1 + members - 1)
+    @pl.when(core == 1)
+    def _():
+        pl.semaphore_wait(ready, 1)
+        for slot in range(len(passed)):
+            pass_on(slot).start()
+
+    @pl.when(jnp.logical_not(leads))
+    def _():
+        pl.semaphore_wait(all_in, 1)
 
     def copy1(k):
         return pltpu.make_async_remote_copy(
@@ -360,13 +405,13 @@
             recv_sem=rt.at[plane], device_id=at_plane(z), device_id_type=MESH,
         )
 
-    def loop(lower, upper, body):
-        def step(z, carry):
-            body(z)
-            return carry
-
-        lax.fori_loop(lower, upper, step, 0)
-
+    @pl.when(core == 1)
+    def _():
+        pass_back().wait_recv()
+
+    steps[pl.ds(core, 1)] = step[...].reshape(1, *step.shape)
+    whole_plane = jnp.sum(jnp.sum(steps[0] + steps[1], axis=1, keepdims=True), axis=0, keepdims=True)
+    plane_time[...] = jnp.broadcast_to(whole_plane, plane_time.shape)
     loop(plane + 1, planes, lambda z: copy_time(z).start())
     got1[pl.ds(place, 1)] = send1[pl.ds(place, 1)]
     for k in range(members):
@@ -483,7 +528,7 @@
             p_re, p_im = e_re[i, here, :], e_im[i, here, :]
             inj[i, here, :LANES] = (p_re * a_re - p_im * a_im).astype(BF16)
             inj[i, here, LANES:] = (p_re * a_im + p_im * a_re).astype(BF16)
-        read = tables[shard, 2 * LANES :, :].astype(F32)
+        read = tables[shard, LANES:, :].astype(F32)
         lane_group = lax.broadcasted_iota(jnp.int32, (CHUNK, LANES), 1) // group_rows
         blocks = [
             jnp.where(lane_group == 2 * inner + g, read[b * CHUNK : (b + 1) * CHUNK], 0.0)
@@ -526,25 +571,40 @@
     loop(plane + 1, planes, lambda z: copy_time(z).wait_send())
     loop(plane + 1, planes, lambda z: copy2(z).wait_send())
 
-
-def mix(tokens, proj, tables, rates, steps, in_gain, out_gain):
+    @pl.when(core == 1)
+    def _():
+        for slot in range(len(passed)):
+            pass_on(slot).wait_send()
+
+    @pl.when(core == 0)
+    def _():
+        pass_back().wait_send()
+
+
+def mix(tokens, proj, decay, frequency, input_map, readout, step, in_gain, out_gain):
     rows, width = tokens.shape
     shards = lax.axis_size("tp")
     planes = lax.axis_size("sp") // 2
     members = 2 * shards
-    tiles = shards * rates.shape[1] // 2
+    pairs = decay.size // LANES
+    tiles = shards * pairs
     vmem = pl.BlockSpec(memory_space=pltpu.VMEM)
     far = pl.BlockSpec(memory_space=pl.ANY)
     table = pltpu.VMEM((tiles, rows, LANES), F32)
     dma = pltpu.SemaphoreType.DMA
+    passed = shards + 3
     return pl.pallas_call(
         mixer_kernel,
         out_shape=jax.ShapeDtypeStruct((rows, shards * LANES), BF16),
-        in_specs=[far, far] + [vmem] * 5,
+        in_specs=[far] * 6 + [vmem] * 3,
         out_specs=vmem,
         scratch_shapes=[
             pltpu.VMEM(tokens.shape, BF16),
-            pltpu.VMEM(proj.shape, BF16),
+            pltpu.VMEM((shards, *proj.shape), BF16),
+            pltpu.VMEM((shards, 2 * LANES, LANES), BF16),
+            pltpu.VMEM((shards, 2 * pairs, LANES), F32),
+            pltpu.VMEM((2, *step.shape), F32),
+            *(pltpu.VMEM(a.shape, F32) for a in (decay, frequency, input_map, readout)),
             pltpu.VMEM(tokens.shape, BF16),
             pltpu.VMEM((shards, rows, LANES), BF16),
             table, table, table, table,
@@ -555,7 +615,6 @@
             pltpu.VMEM((rows, LANES), F32),
             pltpu.VMEM((members, 8, LANES), F32),
             pltpu.VMEM((members, 8, LANES), F32),
-            pltpu.VMEM((4, LANES), F32),
             pltpu.VMEM((planes, 4, LANES), F32),
             pltpu.VMEM((4, LANES), F32),
             pltpu.VMEM((planes, 4, LANES), F32),
@@ -563,36 +622,29 @@
             pltpu.VMEM((planes, 1, LANES), F32),
             pltpu.VMEM((members, 4, LANES), F32),
             pltpu.VMEM((members, 4, LANES), F32),
-            dma((2,)),
+            dma((6,)),
             dma((members,)), dma((members,)),
             dma((planes,)), dma((planes,)),
             dma((planes,)), dma((planes,)),
             dma((members,)), dma((members,)),
+            dma((6,)), dma((6,)), dma((6,)), dma((6,)), dma((3,)), dma((3,)),
+            dma((passed,)), dma((passed,)),
+            pltpu.SemaphoreType.REGULAR,
+            pltpu.SemaphoreType.REGULAR,
         ],
         compiler_params=pltpu.CompilerParams(
-            collective_id=1, has_side_effects=True, vmem_limit_bytes=48 << 20
+            collective_id=0, has_side_effects=True, vmem_limit_bytes=48 << 20
         ),
         name="mixer",
-    )(tokens, proj, tables, rates, steps, in_gain, out_gain)
+    )(tokens, proj, decay, frequency, input_map, readout, step, in_gain, out_gain)
 
 
 def on_device(
     tokens, step, in_gain, in_proj, decay_rate, frequency, input_map, readout, out_gain, out_proj
 ):
-    groups, states = decay_rate.shape
-    lam_re, lam_im = -decay_rate[:, :, None], frequency[:, :, None]
-    size = lam_re * lam_re + lam_im * lam_im
-    b_re = (input_map[0] * lam_re + input_map[1] * lam_im) / size
-    b_im = (input_map[1] * lam_re - input_map[0] * lam_im) / size
-    rows = groups * input_map.shape[-1]
-    push = jnp.stack([b_re, b_re, b_im, b_im]).transpose(1, 3, 0, 2).reshape(rows, 2, 2 * states)
-    push = push.transpose(1, 0, 2).reshape(2 * rows, 2 * states)
-    read = jnp.stack([readout[0], -readout[1]]).transpose(0, 3, 1, 2).reshape(2 * states, rows)
-    tables = jnp.concatenate([push, read], axis=0).astype(BF16)
-    rates = jnp.concatenate([decay_rate, frequency], axis=0).reshape(-1, LANES)
-    proj, tables, rates, steps = gather_over_tp(in_proj, tables, rates, step.reshape(-1, LANES))
     shaped = mix(
-        tokens, proj, tables, rates, steps, in_gain.reshape(1, -1), out_gain.reshape(1, -1)
+        tokens, in_proj, decay_rate, frequency, input_map, readout,
+        step.reshape(-1, LANES), in_gain.reshape(1, -1), out_gain.reshape(1, -1),
     )
     return jnp.dot(shaped, out_proj, preferred_element_type=F32).astype(BF16)
 

time: 90.6 us -> 80.5 us (0.89)
  Pallas kernels: 81.9 us -> 70.5 us
  local copies, waits for them, and re-layouts: 3.16 us -> 7.86 us
  other arithmetic: 3.43 us -> 0 us
    pallas_call x1 -> x0, Pallas kernels: 54.3 us -> none  [gather_over_tp(): pl.pallas_call(gather_kernel, out_shape=(jax.ShapeDtypeStruct((count, *pr...]
    pallas_call x1, Pallas kernels: 27.6 us -> 70.5 us  [mix(): pl.pallas_call(mixer_kernel, out_shape=jax.ShapeDtypeStruct((rows, shards...]
    unnamed x12 -> x19, local copies, waits for them, and re-layouts: 1.74 us -> 7.86 us
    another operation x2 -> x0, other arithmetic: 1.76 us -> none
where the time goes in v2:
time: 80.5 us; the launch traced here: 80.1 us
  Pallas kernels  70.5 us (88%)
  local copies, waits for them, and re-layouts  7.86 us (10%)
  matrix products  1.69 us (2%)
    pallas_call x1, Pallas kernels, mix(): pl.pallas_call(mixer_kernel, out_shape=jax.ShapeDtypeStruct((rows, shards...  70.5 us
    unnamed x19, local copies, waits for them, and re-layouts  7.86 us
    dot_general x1, matrix products, on_device(): return jnp.dot(shaped, out_proj, preferred_element_type=F32).astype(BF16)  1.69 us

profile of v2, /device:TPU:33, one launch (start us, length us, event | category | flops | bytes accessed | tf_op | source)
XLA Modules:
  0.0 80.1 jit_solution(1342577565711661370)
XLA Ops:
  0.0 0.0 copy-start
  0.0 1.3 %copy.11.input_map = f32[2,8,64,16]{3,2,1,0:T(8,128)S(1)} copy(f32[2,8,64,16]{2,3,1,0:T(8,128)} %param.16) | data formatting | bytes 131072 | tf_op args[6]
  1.3 0.0 copy-start.1
  1.3 1.2 %copy-done.1 = bf16[256,2048]{1,0:T(8,128)(2,1)S(1)} copy-done((bf16[256,2048]{1,0:T(8,128)(2,1)S(1)}, bf16[256,2048]{1,0:T(8,128)(2,1)}, u32[]{:S(2)}) %copy-start.1) | copy-done | bytes 1048600
  2.5 0.0 copy-start.2
  2.5 1.0 %copy-done.2 = bf16[2048,128]{1,0:T(8,128)(2,1)S(1)} copy-done((bf16[2048,128]{1,0:T(8,128)(2,1)S(1)}, bf16[2048,128]{1,0:T(8,128)(2,1)}, u32[]{:S(2)}) %copy-start.2) | copy-done | bytes 524312
  3.5 0.0 copy-start.3
  3.5 0.9 %copy-done.3 = f32[2,8,16,64]{3,2,1,0:T(8,128)S(1)} copy-done((f32[2,8,16,64]{3,2,1,0:T(8,128)S(1)}, f32[2,8,16,64]{3,2,1,0:T(8,128)}, u32[]{:S(2)}) %copy-start.3) | copy-done | bytes 65560
  4.4 0.0 copy-start.4
  4.4 0.7 copy-done.4
  5.1 0.0 copy-start.5
  5.1 0.7 copy-done.5
  5.8 0.0 copy-start.6
  5.8 0.7 copy-done.6
  6.5 0.0 copy-start.7
  6.5 0.7 copy-done.7
  7.2 0.0 copy-start.8
  7.2 0.7 copy-done.8
  7.9 70.5 %mixer.1 = bf16[256,512]{1,0:T(8,128)(2,1)S(1)} custom-call(bf16[256,2048]{1,0:T(8,128)(2,1)S(1)} %copy-done.1, bf16[2048,128]{1,0:T(8,128)(2,1)S(1)} %copy-done.2, f32[8,64]{1,0:T(8,128)S(1)} %copy-done.5, f32[8,64]{1,0:T(8,128)S(1)} %copy-done.6, f32[2,8,64,16]{3,2,1,0:T(8,128)S(1)} %copy.11.input_map, f32[2,8,16,64]{3,2,1,0:T(8,128)S(1)} %copy-done.3, ...), custom_call_target="tpu_custom_call" | custom-call | tf_op jit(solution)/shard_map/mixer/pallas_call | solution.py:596
  78.4 0.0 copy-done
  78.4 1.7 %convolution_convert_fusion = bf16[256,2048]{1,0:T(8,128)(2,1)} fusion(bf16[256,512]{1,0:T(8,128)(2,1)S(1)} %mixer.1, bf16[512,2048]{1,0:T(8,128)(2,1)S(1)} %copy-done), kind=kOutput, calls=%fused_computation | convolution fusion | flops 537395200 | bytes 3407872 | tf_op jit(solution)/shard_map/dot_general | solution.py:649
Async XLA Ops:
  0.0 78.4 %copy-start = (bf16[512,2048]{1,0:T(8,128)(2,1)S(1)}, bf16[512,2048]{1,0:T(8,128)(2,1)}, u32[]{:S(2)}) copy-start(bf16[512,2048]{1,0:T(8,128)(2,1)} %param.19) | copy-start | bytes 6291460
  1.3 1.2 %copy-start.1 = (bf16[256,2048]{1,0:T(8,128)(2,1)S(1)}, bf16[256,2048]{1,0:T(8,128)(2,1)}, u32[]{:S(2)}) copy-start(bf16[256,2048]{1,0:T(8,128)(2,1)} %tokens.1) | copy-start | bytes 3145732
  2.5 1.0 %copy-start.2 = (bf16[2048,128]{1,0:T(8,128)(2,1)S(1)}, bf16[2048,128]{1,0:T(8,128)(2,1)}, u32[]{:S(2)}) copy-start(bf16[2048,128]{1,0:T(8,128)(2,1)} %proj.1) | copy-start | bytes 1572868
  3.5 0.9 %copy-start.3 = (f32[2,8,16,64]{3,2,1,0:T(8,128)S(1)}, f32[2,8,16,64]{3,2,1,0:T(8,128)}, u32[]{:S(2)}) copy-start(f32[2,8,16,64]{3,2,1,0:T(8,128)} %readout.1) | copy-start | bytes 196612
  4.4 0.7 copy-start.4
  5.1 0.7 copy-start.5
  5.8 0.7 copy-start.6
  6.5 0.7 copy-start.7
  7.2 0.7 copy-start.8

commit v3 on v2

--- a/solution.py
+++ b/solution.py
@@ -96,14 +96,16 @@
         copy.wait_send()
 
 
-def own_tables(tables, rates, me, decay, frequency, input_map, readout):
+def own_tables(tables, rates, me, decay, frequency, input_map, readout, paired):
     groups, states = decay.shape
-    channels = input_map.shape[-1]
+    channels = input_map.shape[-2]
     pairs = groups // 2
     for g in range(groups):
         lanes = slice((g % 2) * states, (g % 2 + 1) * states)
         rates[me, g // 2 : g // 2 + 1, lanes] = decay[g : g + 1, :]
         rates[me, pairs + g // 2 : pairs + g // 2 + 1, lanes] = frequency[g : g + 1, :]
+        for c in range(2):
+            paired[c, g // 2, :, lanes] = input_map[c, g]
 
     def turned(value):
         size = value.shape[1]
@@ -117,12 +119,11 @@
             precision=lax.Precision.HIGHEST, preferred_element_type=F32,
         )
 
-    maps = [turned(input_map[c].reshape(groups * states, channels)) for c in range(2)]
     for k in range(pairs):
         lam_re = -rates[me, k : k + 1, :]
         lam_im = rates[me, pairs + k : pairs + k + 1, :]
         size = lam_re * lam_re + lam_im * lam_im
-        m_re, m_im = (m[:, k * LANES : (k + 1) * LANES] for m in maps)
+        m_re, m_im = paired[0, k], paired[1, k]
         at = 2 * channels * k
         tables[me, at : at + channels, :] = ((m_re * lam_re + m_im * lam_im) / size).astype(BF16)
         tables[me, at + channels : at + 2 * channels, :] = (
@@ -134,8 +135,9 @@
 
 
 def mixer_kernel(
-    tokens, proj, decay, frequency, input_map, readout, step, in_gain, out_gain, shaped,
-    tok, wide, tables, rates, steps, decay_in, frequency_in, input_map_in, readout_in,
+    tokens, proj, decay, frequency, input_map, readout, step_hbm, in_gain_hbm, out_gain_hbm, shaped,
+    tok, wide, tables, rates, steps, step, in_gain, out_gain,
+    decay_in, frequency_in, input_map_in, readout_in, paired,
     normed, drive, e_re, e_im, g_re, g_im, inj, pushed, total, answer, tau,
     send1, got1, decays, plane_end, plane_got, plane_time, time_got, send3, got3,
     load, s1, r1, s2, r2, st, rt, s3, r3,
@@ -160,7 +162,6 @@
         return {"sp": z * 2 + core}
 
     partner = {"sp": sp + 1 - 2 * core}
-    leads = place == 0
 
     def loop(lower, upper, body):
         def step(z, carry):
@@ -169,29 +170,42 @@
 
         lax.fori_loop(lower, upper, step, 0)
 
+    hub = 1
+    first_chip = me == 0
     barrier = pltpu.get_barrier_semaphore()
 
     def greet(target):
         pl.semaphore_signal(barrier, inc=1, device_id=target, device_id_type=MESH)
 
-    loop(0, plane, lambda z: greet({"sp": 2 * z}))
+    loads = [
+        pltpu.make_async_copy(src, dst, load.at[k])
+        for k, (src, dst) in enumerate(
+            (
+                (tokens, tok),
+                (proj, wide.at[me]),
+                (step_hbm, step),
+                (in_gain_hbm, in_gain),
+                (out_gain_hbm, out_gain),
+            )
+        )
+    ]
 
     @pl.when(core == 1)
     def _():
         for k in range(1, tp_count):
             greet({"tp": lax.rem(me + k, tp_count)})
+
+    @pl.when((core == 0) != first_chip)
+    def _():
         greet(partner)
 
-    @pl.when(jnp.logical_and(jnp.logical_not(leads), place != tp_count))
-    def _():
-        greet({"sp": 2 * plane, "tp": 0})
-
-    loads = [
-        pltpu.make_async_copy(tokens, tok, load.at[0]),
-        pltpu.make_async_copy(proj, wide.at[me], load.at[1]),
-    ]
-    for copy in loads:
-        copy.start()
+    @pl.when(place != hub)
+    def _():
+        greet(member(hub))
+
+    for k in (2, 0, 1, 3, 4):
+        loads[k].start()
+    loop(0, plane, lambda z: greet({"sp": 2 * z, "tp": hub}))
 
     passed = [
         (rates, rates),
@@ -214,10 +228,14 @@
             recv_sem=pass_got.at[slot], device_id=partner, device_id_type=MESH,
         )
 
+    def pass_all():
+        for slot in (0, *range(2, len(passed)), 1):
+            pass_on(slot).start()
+
     @pl.when(core == 1)
     def _():
         inward = [
-            pltpu.make_async_copy(src, dst, load.at[2 + k])
+            pltpu.make_async_copy(src, dst, load.at[len(loads) + k])
             for k, (src, dst) in enumerate(
                 (
                     (decay, decay_in),
@@ -231,30 +249,25 @@
             copy.start()
         for copy in inward:
             copy.wait()
-        own_tables(tables, rates, me, decay_in, frequency_in, input_map_in, readout_in)
+        own_tables(
+            tables, rates, me, decay_in, frequency_in, input_map_in, readout_in, paired
+        )
         loads[1].wait()
-        pl.semaphore_wait(barrier, tp_count - 1)
+        pl.semaphore_wait(barrier, tp_count - jnp.where(first_chip, 1, 0))
         gather_over_tp(
             wide, tables, rates, proj_sent, proj_got, table_sent, table_got, rate_sent, rate_got
         )
 
-    later = 2 * (planes - 1 - plane)
-
-    @pl.when(leads)
-    def _():
-        pl.semaphore_wait(barrier, members - 1 + later)
+    @pl.when(jnp.logical_and(core == 0, first_chip))
+    def _():
+        pl.semaphore_wait(barrier, 1)
         pl.semaphore_signal(ready, inc=1, device_id=partner, device_id_type=MESH)
-        for k in range(1, members):
-            pl.semaphore_signal(all_in, inc=1, device_id=member(k), device_id_type=MESH)
-
-    @pl.when(jnp.logical_and(core == 0, jnp.logical_not(leads)))
-    def _():
-        pl.semaphore_wait(barrier, 1 + later)
-        pl.semaphore_signal(ready, inc=1, device_id=partner, device_id_type=MESH)
-
-    @pl.when(core == 0)
-    def _():
-        pass_back().start()
+
+    loads[2].wait()
+
+    @pl.when(jnp.logical_and(core == 1, jnp.logical_not(first_chip)))
+    def _():
+        pass_all()
 
     row = lax.broadcasted_iota(jnp.int32, (rows, LANES), 0)
     lane = lax.broadcasted_iota(jnp.int32, (rows, LANES), 1)
@@ -268,6 +281,7 @@
         )
     tau[...] = jnp.broadcast_to(column, (rows, LANES))
     loads[0].wait()
+    loads[3].wait()
     strip = 16
 
     def norm(i, carry):
@@ -378,15 +392,25 @@
 
     lax.fori_loop(0, tiles // 2, inject_pair, 0)
 
-    @pl.when(core == 1)
+    @pl.when(jnp.logical_and(core == 1, first_chip))
     def _():
         pl.semaphore_wait(ready, 1)
-        for slot in range(len(passed)):
-            pass_on(slot).start()
-
-    @pl.when(jnp.logical_not(leads))
+        pass_all()
+
+    @pl.when(place == hub)
+    def _():
+        pl.semaphore_wait(barrier, members - 1 + members * (planes - 1 - plane))
+        for k in range(members):
+            if k != hub:
+                pl.semaphore_signal(all_in, inc=1, device_id=member(k), device_id_type=MESH)
+
+    @pl.when(place != hub)
     def _():
         pl.semaphore_wait(all_in, 1)
+
+    @pl.when(core == 0)
+    def _():
+        pass_back().start()
 
     def copy1(k):
         return pltpu.make_async_remote_copy(
@@ -413,6 +437,15 @@
     whole_plane = jnp.sum(jnp.sum(steps[0] + steps[1], axis=1, keepdims=True), axis=0, keepdims=True)
     plane_time[...] = jnp.broadcast_to(whole_plane, plane_time.shape)
     loop(plane + 1, planes, lambda z: copy_time(z).start())
+    p_row = lax.broadcasted_iota(jnp.int32, (rows, rows), 0)
+    p_col = lax.broadcasted_iota(jnp.int32, (rows, rows), 1)
+    lower = jnp.where(p_col <= p_row, 1.0, 0.0).astype(BF16)
+
+    def prefix(i):
+        total[i] = jnp.dot(lower, inj[i], preferred_element_type=F32)
+
+    loop(0, tiles, prefix)
+
     got1[pl.ds(place, 1)] = send1[pl.ds(place, 1)]
     for k in range(members):
         @pl.when(place != k)
@@ -441,15 +474,6 @@
         )
 
     loop(plane + 1, planes, lambda z: copy2(z).start())
-
-    p_row = lax.broadcasted_iota(jnp.int32, (rows, rows), 0)
-    p_col = lax.broadcasted_iota(jnp.int32, (rows, rows), 1)
-    lower = jnp.where(p_col <= p_row, 1.0, 0.0).astype(BF16)
-
-    def prefix(i):
-        total[i] = jnp.dot(lower, inj[i], preferred_element_type=F32)
-
-    loop(0, tiles, prefix)
 
     def time_wait(z):
         pltpu.make_async_remote_copy(
@@ -545,6 +569,8 @@
 
     loop(0, tiles // 2, respond_pair)
 
+    loads[4].wait()
+
     def finish(i):
         here = pl.ds(pl.multiple_of(i * CHUNK, CHUNK), CHUNK)
         values = []
@@ -589,14 +615,14 @@
     pairs = decay.size // LANES
     tiles = shards * pairs
     vmem = pl.BlockSpec(memory_space=pltpu.VMEM)
-    far = pl.BlockSpec(memory_space=pl.ANY)
+    far = pl.BlockSpec(memory_space=pltpu.HBM)
     table = pltpu.VMEM((tiles, rows, LANES), F32)
     dma = pltpu.SemaphoreType.DMA
     passed = shards + 3
     return pl.pallas_call(
         mixer_kernel,
         out_shape=jax.ShapeDtypeStruct((rows, shards * LANES), BF16),
-        in_specs=[far] * 6 + [vmem] * 3,
+        in_specs=[far] * 9,
         out_specs=vmem,
         scratch_shapes=[
             pltpu.VMEM(tokens.shape, BF16),
@@ -604,7 +630,9 @@
             pltpu.VMEM((shards, 2 * LANES, LANES), BF16),
             pltpu.VMEM((shards, 2 * pairs, LANES), F32),
             pltpu.VMEM((2, *step.shape), F32),
+            *(pltpu.VMEM(a.shape, F32) for a in (step, in_gain, out_gain)),
             *(pltpu.VMEM(a.shape, F32) for a in (decay, frequency, input_map, readout)),
+            pltpu.VMEM((2, pairs, input_map.shape[2], LANES), F32),
             pltpu.VMEM(tokens.shape, BF16),
             pltpu.VMEM((shards, rows, LANES), BF16),
             table, table, table, table,
@@ -622,7 +650,7 @@
             pltpu.VMEM((planes, 1, LANES), F32),
             pltpu.VMEM((members, 4, LANES), F32),
             pltpu.VMEM((members, 4, LANES), F32),
-            dma((6,)),
+            dma((9,)),
             dma((members,)), dma((members,)),
             dma((planes,)), dma((planes,)),
             dma((planes,)), dma((planes,)),
@@ -636,14 +664,19 @@
             collective_id=0, has_side_effects=True, vmem_limit_bytes=48 << 20
         ),
         name="mixer",
-    )(tokens, proj, decay, frequency, input_map, readout, step, in_gain, out_gain)
+    )(
+        *(
+            pltpu.with_memory_space_constraint(a, pltpu.HBM)
+            for a in (tokens, proj, decay, frequency, input_map, readout, step, in_gain, out_gain)
+        )
+    )
 
 
 def on_device(
     tokens, step, in_gain, in_proj, decay_rate, frequency, input_map, readout, out_gain, out_proj
 ):
     shaped = mix(
-        tokens, in_proj, decay_rate, frequency, input_map, readout,
+        tokens, in_proj, decay_rate, frequency, jnp.swapaxes(input_map, 2, 3), readout,
         step.reshape(-1, LANES), in_gain.reshape(1, -1), out_gain.reshape(1, -1),
     )
     return jnp.dot(shaped, out_proj, preferred_element_type=F32).astype(BF16)

time: 80.5 us -> 66.2 us (0.82)
  local copies, waits for them, and re-layouts: 7.86 us -> 0.01 us
  Pallas kernels: 70.5 us -> 64.3 us
    unnamed x19 -> x2, local copies, waits for them, and re-layouts: 7.86 us -> 0.01 us
    pallas_call x1, Pallas kernels: 70.5 us -> 64.3 us  [mix(): pl.pallas_call(mixer_kernel, out_shape=jax.ShapeDtypeStruct((rows, shards...]
where the time goes in v3:
time: 66.2 us; the launch traced here: 66 us
  Pallas kernels  64.3 us (97%)
  matrix products  1.69 us (3%)
    pallas_call x1, Pallas kernels, mix(): pl.pallas_call(mixer_kernel, out_shape=jax.ShapeDtypeStruct((rows, shards...  64.3 us
    dot_general x1, matrix products, on_device(): return jnp.dot(shaped, out_proj, preferred_element_type=F32).astype(BF16)  1.69 us

profile of v3, /device:TPU:33, one launch (start us, length us, event | category | flops | bytes accessed | tf_op | source)
XLA Modules:
  0.0 66.0 jit_solution(16558745768660178581)
XLA Ops:
  0.0 0.0 copy-start
  0.0 64.3 %mixer.1 = bf16[256,512]{1,0:T(8,128)(2,1)S(1)} custom-call(bf16[256,2048]{1,0:T(8,128)(2,1)} %tokens.1, bf16[2048,128]{1,0:T(8,128)(2,1)} %proj.1, f32[8,64]{1,0:T(8,128)} %decay.1, f32[8,64]{1,0:T(8,128)} %frequency.1, f32[2,8,16,64]{3,2,1,0:T(8,128)} %bitcast.6, f32[2,8,16,64]{3,2,1,0:T(8,128)} %readout.1, f32[8,128]{1,0:T(8,128)} %bitcast.8, ...), custom_call_target="tpu_custom_call" | custom-call | tf_op jit(solution)/shard_map/mixer/pallas_call | solution.py:622
  64.3 0.0 copy-done
  64.3 1.7 %convolution_convert_fusion = bf16[256,2048]{1,0:T(8,128)(2,1)} fusion(bf16[256,512]{1,0:T(8,128)(2,1)S(1)} %mixer.1, bf16[512,2048]{1,0:T(8,128)(2,1)S(1)} %copy-done), kind=kOutput, calls=%fused_computation | convolution fusion | flops 537395200 | bytes 3407872 | tf_op jit(solution)/shard_map/dot_general | solution.py:682
Async XLA Ops:
  0.0 64.3 %copy-start = (bf16[512,2048]{1,0:T(8,128)(2,1)S(1)}, bf16[512,2048]{1,0:T(8,128)(2,1)}, u32[]{:S(2)}) copy-start(bf16[512,2048]{1,0:T(8,128)(2,1)} %param.19) | copy-start | bytes 6291460

commit v4 on v3

--- a/solution.py
+++ b/solution.py
@@ -12,8 +12,9 @@
 MESH = pl.DeviceIdType.MESH
 LANES = 128
 CHUNK = 64
+BLOCK = 8
 SIN = (6.283182782944718, -41.34141729070845, 81.59606953187966, -76.57887013158442, 41.19977042473147, -12.262090350994187)
-COS = (0.9999999888727491, -19.7392044313539, 64.939113609812, -85.45006239525888, 60.16694808625918, -25.96486025322117, 6.5245930831162795)
+COS = (0.9999992033069715, -19.738978121285577, 64.92856232184074, -85.27029302060335, 58.78321908130333, -21.057556163478825)
 TURN = np.float32(1.0 / (2.0 * np.pi))
 TURN_LOW = np.float32(1.0 / (2.0 * np.pi) - float(TURN))
 
@@ -43,7 +44,7 @@
     whole = high * times
     part = (whole - jnp.round(whole)) + low * times
     square = part * part
-    return polynomial(square, COS), polynomial(square, SIN) * part
+    return polynomial(square, COS), polynomial(square, [-c for c in SIN]) * part
 
 
 def gather_over_tp(wide, tables, rates, proj_sent, proj_got, table_sent, table_got, rate_sent, rate_got):
@@ -106,43 +107,34 @@
         rates[me, pairs + g // 2 : pairs + g // 2 + 1, lanes] = frequency[g : g + 1, :]
         for c in range(2):
             paired[c, g // 2, :, lanes] = input_map[c, g]
-
-    def turned(value):
-        size = value.shape[1]
-        unit = jnp.where(
-            lax.broadcasted_iota(jnp.int32, (size, size), 0)
-            == lax.broadcasted_iota(jnp.int32, (size, size), 1),
-            1.0, 0.0,
-        ).astype(F32)
-        return lax.dot_general(
-            unit, value, (((1,), (1,)), ((), ())),
-            precision=lax.Precision.HIGHEST, preferred_element_type=F32,
-        )
-
+            paired[2 + c, g // 2, :, lanes] = readout[c, g]
     for k in range(pairs):
         lam_re = -rates[me, k : k + 1, :]
         lam_im = rates[me, pairs + k : pairs + k + 1, :]
         size = lam_re * lam_re + lam_im * lam_im
         m_re, m_im = paired[0, k], paired[1, k]
-        at = 2 * channels * k
-        tables[me, at : at + channels, :] = ((m_re * lam_re + m_im * lam_im) / size).astype(BF16)
-        tables[me, at + channels : at + 2 * channels, :] = (
-            (m_im * lam_re - m_re * lam_im) / size
-        ).astype(BF16)
-    for c, sign in ((0, 1.0), (1, -1.0)):
-        value = sign * turned(readout[c].reshape(groups * channels, states))
-        tables[me, LANES + c * states : LANES + (c + 1) * states, :] = value.astype(BF16)
+        for b, value in enumerate(
+            (
+                (m_re * lam_re + m_im * lam_im) / size,
+                (m_im * lam_re - m_re * lam_im) / size,
+                paired[2, k],
+                -paired[3, k],
+            )
+        ):
+            at = (b // 2) * LANES + (2 * k + b % 2) * channels
+            tables[me, at : at + channels, :] = value.astype(BF16)
 
 
 def mixer_kernel(
     tokens, proj, decay, frequency, input_map, readout, step_hbm, in_gain_hbm, out_gain_hbm, shaped,
     tok, wide, tables, rates, steps, step, in_gain, out_gain,
     decay_in, frequency_in, input_map_in, readout_in, paired,
-    normed, drive, e_re, e_im, g_re, g_im, inj, pushed, total, answer, tau,
+    normed, drive, q_re, q_im, g_re, g_im, inj, back, pushed, answer, tau,
     send1, got1, decays, plane_end, plane_got, plane_time, time_got, send3, got3,
+    block_end, block_got, block_in,
     load, s1, r1, s2, r2, st, rt, s3, r3,
     proj_sent, proj_got, table_sent, table_got, rate_sent, rate_got, pass_sent, pass_got,
-    ready, all_in,
+    sb, rb, ready, all_in,
 ):
     rows = tok.shape[0]
     tp_count, sp_count = lax.axis_size("tp"), lax.axis_size("sp")
@@ -150,8 +142,11 @@
     members = 2 * tp_count
     me, sp = lax.axis_index("tp"), lax.axis_index("sp")
     core, plane = lax.rem(sp, 2), sp // 2
+    first = plane - lax.rem(plane, BLOCK)
+    stop = jnp.minimum(first + BLOCK, planes)
+    reach = jnp.where(plane == stop - 1, jnp.minimum(stop + BLOCK, planes), stop)
     place = core * tp_count + me
-    tiles = e_re.shape[0]
+    tiles = q_re.shape[0]
     per_shard = tiles // tp_count
     shards = tp_count
 
@@ -170,7 +165,7 @@
 
         lax.fori_loop(lower, upper, step, 0)
 
-    hub = 1
+    hub, gate = 1, 2
     first_chip = me == 0
     barrier = pltpu.get_barrier_semaphore()
 
@@ -205,7 +200,15 @@
 
     for k in (2, 0, 1, 3, 4):
         loads[k].start()
-    loop(0, plane, lambda z: greet({"sp": 2 * z, "tp": hub}))
+
+    def plane_in():
+        pl.semaphore_wait(barrier, members - 1)
+        greet(member(gate))
+        loop(jnp.maximum(first - 1, 0), plane, lambda z: greet({"sp": 2 * z, "tp": gate}))
+
+    @pl.when(jnp.logical_and(place == hub, plane > 0))
+    def _():
+        plane_in()
 
     passed = [
         (rates, rates),
@@ -296,27 +299,30 @@
     def _():
         pass_on(0).wait_recv()
 
-    first_row = lax.broadcasted_iota(jnp.int32, (CHUNK, LANES), 0) == 0
+    first_row = lax.broadcasted_iota(jnp.int32, (8, LANES), 0) == 0
+
+    def rate_row(i):
+        return rates[i // per_shard, pl.ds(lax.rem(i, per_shard), 1), :]
+
+    def turn_rows(i):
+        return turns_of(rates[i // per_shard, pl.ds(per_shard + lax.rem(i, per_shard), 1), :])
 
     def tables_of(i, carry):
-        shard, inner = i // per_shard, lax.rem(i, per_shard)
-        rate = rates[shard, pl.ds(inner, 1), :]
-        high, low = turns_of(rates[shard, pl.ds(per_shard + inner, 1), :])
-        before_re = jnp.ones((CHUNK, LANES), F32)
-        before_im = jnp.zeros((CHUNK, LANES), F32)
+        rate, (high, low) = rate_row(i), turn_rows(i)
+        before = [jnp.ones((8, LANES), F32), jnp.zeros((8, LANES), F32)]
         for c in range(0, rows, CHUNK):
             here = pl.ds(c, CHUNK)
             times = tau[here, :]
-            cosine, sine = rotation(high, low, times)
-            exponent = rate * times
-            shrink, grow = jnp.exp(-exponent), jnp.exp(exponent)
-            e_re[i, here, :] = shrink * cosine
-            e_im[i, here, :] = shrink * sine
-            q_re, q_im = grow * cosine, -(grow * sine)
-            turned_re, turned_im = pltpu.roll(q_re, 1, 0), pltpu.roll(q_im, 1, 0)
-            g_re[i, here, :] = jnp.where(first_row, before_re, turned_re) - q_re
-            g_im[i, here, :] = jnp.where(first_row, before_im, turned_im) - q_im
-            before_re, before_im = turned_re, turned_im
+            grow = jnp.exp(rate * times)
+            for b, (part, q_ref, g_ref) in enumerate(
+                zip(rotation(high, low, times), (q_re, q_im), (g_re, g_im))
+            ):
+                value = grow * part
+                q_ref[i, here, :] = value
+                turned = pltpu.roll(value, 1, 0)
+                head = jnp.where(first_row, before[b], turned[:8])
+                before[b] = turned[:8]
+                g_ref[i, here, :] = jnp.concatenate([head, turned[8:]], axis=0) - value
         return carry
 
     lax.fori_loop(0, tiles, tables_of, 0)
@@ -340,27 +346,25 @@
     k_lane = lax.broadcasted_iota(jnp.int32, (LANES, LANES), 1)
     group_rows = LANES // (2 * per_shard)
 
+    def own_groups(inner):
+        return k_row // group_rows == 2 * inner + k_lane // (LANES // 2)
+
+    def compact(shard, block):
+        at = pl.multiple_of(block * group_rows, group_rows)
+        return tables[shard, pl.ds(at, group_rows), :].astype(F32)
+
+    def widened(value, mask):
+        return jnp.where(mask, jnp.concatenate([value] * (LANES // group_rows), axis=0), 0.0).astype(
+            BF16
+        )
+
+    def spread(shard, block, mask):
+        return widened(compact(shard, block), mask)
+
     def inject(i, half):
         shard, inner = i // per_shard, lax.rem(i, per_shard)
-        mask = k_row // group_rows == 2 * inner + k_lane // CHUNK
-        push = [
-            jnp.where(
-                mask,
-                jnp.concatenate(
-                    [
-                        tables[
-                            shard,
-                            pl.ds(pl.multiple_of((2 * inner + b) * group_rows, group_rows), group_rows),
-                            :,
-                        ].astype(F32)
-                    ]
-                    * (LANES // group_rows),
-                    axis=0,
-                ),
-                0.0,
-            ).astype(BF16)
-            for b in range(2)
-        ]
+        mask = own_groups(inner)
+        push = [spread(shard, 2 * inner + b, mask) for b in range(2)]
         pushed[...] = jnp.dot(
             drive[shard], jnp.concatenate(push, axis=1), preferred_element_type=F32
         )
@@ -378,7 +382,8 @@
             inj[i, here, LANES:] = w_im.astype(BF16)
         t_re = jnp.sum(sum_re, axis=0, keepdims=True)
         t_im = jnp.sum(sum_im, axis=0, keepdims=True)
-        d_re, d_im = e_re[i, rows - 1 : rows, :], e_im[i, rows - 1 : rows, :]
+        fade = jnp.exp(-2.0 * (rate_row(i) * tau[rows - 1 : rows, :]))
+        d_re, d_im = q_re[i, rows - 1 : rows, :] * fade, -(q_im[i, rows - 1 : rows, :] * fade)
         part = i // 2
         send1[part, half : half + 1, :] = d_re * t_re - d_im * t_im
         send1[part, 2 + half : 3 + half, :] = d_re * t_im + d_im * t_re
@@ -397,14 +402,18 @@
         pl.semaphore_wait(ready, 1)
         pass_all()
 
-    @pl.when(place == hub)
-    def _():
-        pl.semaphore_wait(barrier, members - 1 + members * (planes - 1 - plane))
+    @pl.when(jnp.logical_and(place == hub, plane == 0))
+    def _():
+        plane_in()
+
+    @pl.when(place == gate)
+    def _():
+        pl.semaphore_wait(barrier, reach - plane)
         for k in range(members):
-            if k != hub:
+            if k != gate:
                 pl.semaphore_signal(all_in, inc=1, device_id=member(k), device_id_type=MESH)
 
-    @pl.when(place != hub)
+    @pl.when(place != gate)
     def _():
         pl.semaphore_wait(all_in, 1)
 
@@ -436,15 +445,44 @@
     steps[pl.ds(core, 1)] = step[...].reshape(1, *step.shape)
     whole_plane = jnp.sum(jnp.sum(steps[0] + steps[1], axis=1, keepdims=True), axis=0, keepdims=True)
     plane_time[...] = jnp.broadcast_to(whole_plane, plane_time.shape)
-    loop(plane + 1, planes, lambda z: copy_time(z).start())
+    loop(plane + 1, stop, lambda z: copy_time(z).start())
     p_row = lax.broadcasted_iota(jnp.int32, (rows, rows), 0)
     p_col = lax.broadcasted_iota(jnp.int32, (rows, rows), 1)
     lower = jnp.where(p_col <= p_row, 1.0, 0.0).astype(BF16)
 
-    def prefix(i):
-        total[i] = jnp.dot(lower, inj[i], preferred_element_type=F32)
-
-    loop(0, tiles, prefix)
+    blocks = LANES // group_rows
+
+    def across(left, right):
+        return lax.dot_general(
+            left, right, (((1,), (1,)), ((), ())), preferred_element_type=F32
+        )
+
+    def prefix(i, first):
+        shard, inner = i // per_shard, lax.rem(i, per_shard)
+        pushed[...] = jnp.dot(lower, inj[i], preferred_element_type=F32)
+        rate = rate_row(i)
+        for c in range(0, rows, CHUNK):
+            here = pl.ds(c, CHUNK)
+            fade = jnp.exp(-2.0 * (rate * tau[here, :]))
+            e_re, e_im = q_re[i, here, :] * fade, -(q_im[i, here, :] * fade)
+            a_re, a_im = pushed[here, :LANES], pushed[here, LANES:]
+            back[i, here, :LANES] = e_re.astype(BF16)
+            back[i, here, LANES:] = e_im.astype(BF16)
+            inj[i, here, :LANES] = (e_re * a_re - e_im * a_im).astype(BF16)
+            inj[i, here, LANES:] = (e_re * a_im + e_im * a_re).astype(BF16)
+        mask = own_groups(inner)
+        read = [spread(shard, blocks + 2 * inner + b, mask) for b in range(2)]
+        value = across(inj[i], jnp.concatenate(read, axis=1))
+        if first:
+            answer[shard] = value
+        else:
+            answer[shard] += value
+
+    def prefixes(shard):
+        for inner in range(per_shard):
+            prefix(shard * per_shard + inner, inner == 0)
+
+    loop(0, shards, prefixes)
 
     got1[pl.ds(place, 1)] = send1[pl.ds(place, 1)]
     for k in range(members):
@@ -473,7 +511,7 @@
             recv_sem=r2.at[plane], device_id=at_plane(z), device_id_type=MESH,
         )
 
-    loop(plane + 1, planes, lambda z: copy2(z).start())
+    loop(plane + 1, stop, lambda z: copy2(z).start())
 
     def time_wait(z):
         pltpu.make_async_remote_copy(
@@ -481,21 +519,19 @@
             device_id=at_plane(z), device_id_type=MESH,
         ).wait_recv()
 
-    loop(0, plane, time_wait)
+    loop(first, plane, time_wait)
 
     def plane_decay(z):
         times = jnp.broadcast_to(time_got[z], (1, LANES))
         for half in range(2):
             i = 2 * place + half
-            shard, inner = i // per_shard, lax.rem(i, per_shard)
-            rate = rates[shard, pl.ds(inner, 1), :]
-            high, low = turns_of(rates[shard, pl.ds(per_shard + inner, 1), :])
+            rate, (high, low) = rate_row(i), turn_rows(i)
             cosine, sine = rotation(high, low, times)
             shrink = jnp.exp(-(rate * times))
             decays[z, half : half + 1, :] = shrink * cosine
-            decays[z, 2 + half : 3 + half, :] = shrink * sine
-
-    loop(0, plane, plane_decay)
+            decays[z, 2 + half : 3 + half, :] = -(shrink * sine)
+
+    loop(first, plane, plane_decay)
 
     def end_wait(z):
         pltpu.make_async_remote_copy(
@@ -503,7 +539,7 @@
             device_id=at_plane(z), device_id_type=MESH,
         ).wait_recv()
 
-    loop(0, plane, end_wait)
+    loop(first, plane, end_wait)
 
     def earlier(z, carry):
         re, im = carry
@@ -513,7 +549,32 @@
             d[0:2] * im + d[2:4] * re + end[2:4],
         )
 
-    re, im = lax.fori_loop(0, plane, earlier, (nothing, nothing))
+    def copy_block(z):
+        return pltpu.make_async_remote_copy(
+            src_ref=block_end, dst_ref=block_got, send_sem=sb.at[z], recv_sem=rb,
+            device_id=at_plane(z), device_id_type=MESH,
+        )
+
+    @pl.when(first == 0)
+    def _():
+        block_in[...] = jnp.zeros_like(block_in)
+
+    @pl.when(first > 0)
+    def _():
+        copy_block(plane).wait_recv()
+        block_in[...] = block_got[...]
+
+    re, im = lax.fori_loop(first, plane, earlier, (block_in[0:2, :], block_in[2:4, :]))
+
+    @pl.when(reach > stop)
+    def _():
+        after_re, after_im = re, im
+        for k in range(members):
+            after_re, after_im = advance(k, after_re, after_im)
+        block_end[0:2, :] = after_re
+        block_end[2:4, :] = after_im
+
+    loop(stop, reach, lambda z: copy_block(z).start())
     for k in range(members):
         send3[k, 0:2, :] = re
         send3[k, 2:4, :] = im
@@ -539,35 +600,23 @@
                 device_id=member(k), device_id_type=MESH,
             ).wait_recv()
 
-    answer[...] = jnp.zeros_like(answer)
-
-    def respond(i, half):
-        shard, inner = i // per_shard, lax.rem(i, per_shard)
-        part = i // 2
-        in_re = got3[part, half : half + 1, :]
-        in_im = got3[part, 2 + half : 3 + half, :]
-        for c in range(0, rows, CHUNK):
-            here = pl.ds(c, CHUNK)
-            a_re, a_im = total[i, here, :LANES] + in_re, total[i, here, LANES:] + in_im
-            p_re, p_im = e_re[i, here, :], e_im[i, here, :]
-            inj[i, here, :LANES] = (p_re * a_re - p_im * a_im).astype(BF16)
-            inj[i, here, LANES:] = (p_re * a_im + p_im * a_re).astype(BF16)
-        read = tables[shard, LANES:, :].astype(F32)
-        lane_group = lax.broadcasted_iota(jnp.int32, (CHUNK, LANES), 1) // group_rows
-        blocks = [
-            jnp.where(lane_group == 2 * inner + g, read[b * CHUNK : (b + 1) * CHUNK], 0.0)
-            for b in range(2)
-            for g in range(2)
-        ]
-        answer[shard] += jnp.dot(
-            inj[i], jnp.concatenate(blocks, axis=0).astype(BF16), preferred_element_type=F32
-        )
-
-    def respond_pair(part):
-        respond(2 * part, 0)
-        respond(2 * part + 1, 1)
-
-    loop(0, tiles // 2, respond_pair)
+    def respond(shard):
+        value = answer[shard]
+        for inner in range(per_shard):
+            i = shard * per_shard + inner
+            part, half = i // 2, inner % 2
+            in_re = got3[part, half : half + 1, :]
+            in_im = got3[part, 2 + half : 3 + half, :]
+            c_re, c_im = (compact(shard, blocks + 2 * inner + b) for b in range(2))
+            mask = own_groups(inner)
+            read = [
+                widened(c_re * in_re + c_im * in_im, mask),
+                widened(c_im * in_re - c_re * in_im, mask),
+            ]
+            value += across(back[i], jnp.concatenate(read, axis=1))
+        answer[shard] = value
+
+    loop(0, shards, respond)
 
     loads[4].wait()
 
@@ -594,8 +643,9 @@
         def _():
             copy1(k).wait_send()
             copy3(k).wait_send()
-    loop(plane + 1, planes, lambda z: copy_time(z).wait_send())
-    loop(plane + 1, planes, lambda z: copy2(z).wait_send())
+    loop(plane + 1, stop, lambda z: copy_time(z).wait_send())
+    loop(plane + 1, stop, lambda z: copy2(z).wait_send())
+    loop(stop, reach, lambda z: copy_block(z).wait_send())
 
     @pl.when(core == 1)
     def _():
@@ -632,13 +682,13 @@
             pltpu.VMEM((2, *step.shape), F32),
             *(pltpu.VMEM(a.shape, F32) for a in (step, in_gain, out_gain)),
             *(pltpu.VMEM(a.shape, F32) for a in (decay, frequency, input_map, readout)),
-            pltpu.VMEM((2, pairs, input_map.shape[2], LANES), F32),
+            pltpu.VMEM((4, pairs, input_map.shape[2], LANES), F32),
             pltpu.VMEM(tokens.shape, BF16),
             pltpu.VMEM((shards, rows, LANES), BF16),
             table, table, table, table,
             pltpu.VMEM((tiles, rows, 2 * LANES), BF16),
+            pltpu.VMEM((tiles, rows, 2 * LANES), BF16),
             pltpu.VMEM((rows, 2 * LANES), F32),
-            pltpu.VMEM((tiles, rows, 2 * LANES), F32),
             pltpu.VMEM((shards, rows, LANES), F32),
             pltpu.VMEM((rows, LANES), F32),
             pltpu.VMEM((members, 8, LANES), F32),
@@ -650,6 +700,9 @@
             pltpu.VMEM((planes, 1, LANES), F32),
             pltpu.VMEM((members, 4, LANES), F32),
             pltpu.VMEM((members, 4, LANES), F32),
+            pltpu.VMEM((4, LANES), F32),
+            pltpu.VMEM((4, LANES), F32),
+            pltpu.VMEM((4, LANES), F32),
             dma((9,)),
             dma((members,)), dma((members,)),
             dma((planes,)), dma((planes,)),
@@ -657,6 +710,7 @@
             dma((members,)), dma((members,)),
             dma((6,)), dma((6,)), dma((6,)), dma((6,)), dma((3,)), dma((3,)),
             dma((passed,)), dma((passed,)),
+            dma((planes,)), dma,
             pltpu.SemaphoreType.REGULAR,
             pltpu.SemaphoreType.REGULAR,
         ],

time: 66.2 us -> 64 us (0.967)
  Pallas kernels: 64.3 us -> 62.2 us
    pallas_call x1, Pallas kernels: 64.3 us -> 62.2 us  [mix(): pl.pallas_call(mixer_kernel, out_shape=jax.ShapeDtypeStruct((rows, shards...]
where the time goes in v4:
time: 64 us; the launch traced here: 63.9 us
  Pallas kernels  62.2 us (97%)
  matrix products  1.69 us (3%)
    pallas_call x1, Pallas kernels, mix(): pl.pallas_call(mixer_kernel, out_shape=jax.ShapeDtypeStruct((rows, shards...  62.2 us
    dot_general x1, matrix products, on_device(): return jnp.dot(shaped, out_proj, preferred_element_type=F32).astype(BF16)  1.69 us

profile of v4, /device:TPU:33, one launch (start us, length us, event | category | flops | bytes accessed | tf_op | source)
XLA Modules:
  0.0 63.9 jit_solution(11151199039420203769)
XLA Ops:
  0.0 0.0 copy-start
  0.0 62.2 %mixer.1 = bf16[256,512]{1,0:T(8,128)(2,1)S(1)} custom-call(bf16[256,2048]{1,0:T(8,128)(2,1)} %tokens.1, bf16[2048,128]{1,0:T(8,128)(2,1)} %proj.1, f32[8,64]{1,0:T(8,128)} %decay.1, f32[8,64]{1,0:T(8,128)} %frequency.1, f32[2,8,16,64]{3,2,1,0:T(8,128)} %bitcast.6, f32[2,8,16,64]{3,2,1,0:T(8,128)} %readout.1, f32[8,128]{1,0:T(8,128)} %bitcast.8, ...), custom_call_target="tpu_custom_call" | custom-call | tf_op jit(solution)/shard_map/mixer/pallas_call | solution.py:672
  62.2 0.0 copy-done
  62.2 1.7 %convolution_convert_fusion = bf16[256,2048]{1,0:T(8,128)(2,1)} fusion(bf16[256,512]{1,0:T(8,128)(2,1)S(1)} %mixer.1, bf16[512,2048]{1,0:T(8,128)(2,1)S(1)} %copy-done), kind=kOutput, calls=%fused_computation | convolution fusion | flops 537395200 | bytes 3407872 | tf_op jit(solution)/shard_map/dot_general | solution.py:736
Async XLA Ops:
  0.0 62.2 %copy-start = (bf16[512,2048]{1,0:T(8,128)(2,1)S(1)}, bf16[512,2048]{1,0:T(8,128)(2,1)}, u32[]{:S(2)}) copy-start(bf16[512,2048]{1,0:T(8,128)(2,1)} %param.19) | copy-start | bytes 6291460

commit v5 on v4

--- a/solution.py
+++ b/solution.py
@@ -12,7 +12,7 @@
 MESH = pl.DeviceIdType.MESH
 LANES = 128
 CHUNK = 64
-BLOCK = 8
+BLOCK = 4
 SIN = (6.283182782944718, -41.34141729070845, 81.59606953187966, -76.57887013158442, 41.19977042473147, -12.262090350994187)
 COS = (0.9999992033069715, -19.738978121285577, 64.92856232184074, -85.27029302060335, 58.78321908130333, -21.057556163478825)
 TURN = np.float32(1.0 / (2.0 * np.pi))
@@ -285,16 +285,14 @@
     tau[...] = jnp.broadcast_to(column, (rows, LANES))
     loads[0].wait()
     loads[3].wait()
-    strip = 16
-
-    def norm(i, carry):
+    strip = rows // tiles
+
+    def norm(i):
         here = pl.ds(pl.multiple_of(i * strip, strip), strip)
         value = tok[here, :].astype(F32)
         scale = lax.rsqrt(jnp.mean(value * value, axis=1, keepdims=True) + 1e-06)
         normed[here, :] = (value * scale * in_gain[...]).astype(BF16)
-        return carry
-
-    lax.fori_loop(0, rows // strip, norm, 0)
+
     @pl.when(core == 0)
     def _():
         pass_on(0).wait_recv()
@@ -308,6 +306,7 @@
         return turns_of(rates[i // per_shard, pl.ds(per_shard + lax.rem(i, per_shard), 1), :])
 
     def tables_of(i, carry):
+        norm(i)
         rate, (high, low) = rate_row(i), turn_rows(i)
         before = [jnp.ones((8, LANES), F32), jnp.zeros((8, LANES), F32)]
         for c in range(0, rows, CHUNK):
@@ -361,18 +360,20 @@
     def spread(shard, block, mask):
         return widened(compact(shard, block), mask)
 
-    def inject(i, half):
+    def push_through(i, half):
         shard, inner = i // per_shard, lax.rem(i, per_shard)
         mask = own_groups(inner)
         push = [spread(shard, 2 * inner + b, mask) for b in range(2)]
-        pushed[...] = jnp.dot(
+        pushed[half] = jnp.dot(
             drive[shard], jnp.concatenate(push, axis=1), preferred_element_type=F32
         )
+
+    def inject(i, half):
         sum_re = jnp.zeros((CHUNK, LANES), F32)
         sum_im = jnp.zeros((CHUNK, LANES), F32)
         for c in range(0, rows, CHUNK):
             here = pl.ds(c, CHUNK)
-            u_re, u_im = pushed[here, :LANES], pushed[here, LANES:]
+            u_re, u_im = pushed[half, here, :LANES], pushed[half, here, LANES:]
             a_re, a_im = g_re[i, here, :], g_im[i, here, :]
             w_re = a_re * u_re - a_im * u_im
             w_im = a_re * u_im + a_im * u_re
@@ -391,6 +392,8 @@
         send1[part, 6 + half : 7 + half, :] = d_im
 
     def inject_pair(part, carry):
+        push_through(2 * part, 0)
+        push_through(2 * part + 1, 1)
         inject(2 * part, 0)
         inject(2 * part + 1, 1)
         return carry
@@ -457,15 +460,15 @@
             left, right, (((1,), (1,)), ((), ())), preferred_element_type=F32
         )
 
-    def prefix(i, first):
+    def prefix(i, slot, first):
         shard, inner = i // per_shard, lax.rem(i, per_shard)
-        pushed[...] = jnp.dot(lower, inj[i], preferred_element_type=F32)
+        pushed[slot] = jnp.dot(lower, inj[i], preferred_element_type=F32)
         rate = rate_row(i)
         for c in range(0, rows, CHUNK):
             here = pl.ds(c, CHUNK)
             fade = jnp.exp(-2.0 * (rate * tau[here, :]))
             e_re, e_im = q_re[i, here, :] * fade, -(q_im[i, here, :] * fade)
-            a_re, a_im = pushed[here, :LANES], pushed[here, LANES:]
+            a_re, a_im = pushed[slot, here, :LANES], pushed[slot, here, LANES:]
             back[i, here, :LANES] = e_re.astype(BF16)
             back[i, here, LANES:] = e_im.astype(BF16)
             inj[i, here, :LANES] = (e_re * a_re - e_im * a_im).astype(BF16)
@@ -480,9 +483,7 @@
 
     def prefixes(shard):
         for inner in range(per_shard):
-            prefix(shard * per_shard + inner, inner == 0)
-
-    loop(0, shards, prefixes)
+            prefix(shard * per_shard + inner, inner % 2, inner == 0)
 
     got1[pl.ds(place, 1)] = send1[pl.ds(place, 1)]
     for k in range(members):
@@ -512,6 +513,10 @@
         )
 
     loop(plane + 1, stop, lambda z: copy2(z).start())
+
+    @pl.when(plane > 0)
+    def _():
+        loop(0, shards, prefixes)
 
     def time_wait(z):
         pltpu.make_async_remote_copy(
@@ -591,6 +596,11 @@
         @pl.when(place != k)
         def _():
             copy3(k).start()
+
+    @pl.when(plane == 0)
+    def _():
+        loop(0, shards, prefixes)
+
     got3[pl.ds(place, 1)] = send3[pl.ds(place, 1)]
     for k in range(members):
         @pl.when(place != k)
@@ -688,7 +698,7 @@
             table, table, table, table,
             pltpu.VMEM((tiles, rows, 2 * LANES), BF16),
             pltpu.VMEM((tiles, rows, 2 * LANES), BF16),
-            pltpu.VMEM((rows, 2 * LANES), F32),
+            pltpu.VMEM((2, rows, 2 * LANES), F32),
             pltpu.VMEM((shards, rows, LANES), F32),
             pltpu.VMEM((rows, LANES), F32),
             pltpu.VMEM((members, 8, LANES), F32),

time: 64 us -> 62.3 us (0.973)
  Pallas kernels: 62.2 us -> 60.5 us
    pallas_call x1, Pallas kernels: 62.2 us -> 60.5 us  [mix(): pl.pallas_call(mixer_kernel, out_shape=jax.ShapeDtypeStruct((rows, shards...]
where the time goes in v5:
time: 62.3 us; the launch traced here: 62.2 us
  Pallas kernels  60.5 us (97%)
  matrix products  1.69 us (3%)
    pallas_call x1, Pallas kernels, mix(): pl.pallas_call(mixer_kernel, out_shape=jax.ShapeDtypeStruct((rows, shards...  60.5 us
    dot_general x1, matrix products, on_device(): return jnp.dot(shaped, out_proj, preferred_element_type=F32).astype(BF16)  1.69 us

profile of v5, /device:TPU:33, one launch (start us, length us, event | category | flops | bytes accessed | tf_op | source)
XLA Modules:
  0.0 62.2 jit_solution(5088031362104984474)
XLA Ops:
  0.0 0.0 copy-start
  0.0 60.5 %mixer.1 = bf16[256,512]{1,0:T(8,128)(2,1)S(1)} custom-call(bf16[256,2048]{1,0:T(8,128)(2,1)} %tokens.1, bf16[2048,128]{1,0:T(8,128)(2,1)} %proj.1, f32[8,64]{1,0:T(8,128)} %decay.1, f32[8,64]{1,0:T(8,128)} %frequency.1, f32[2,8,16,64]{3,2,1,0:T(8,128)} %bitcast.6, f32[2,8,16,64]{3,2,1,0:T(8,128)} %readout.1, f32[8,128]{1,0:T(8,128)} %bitcast.8, ...), custom_call_target="tpu_custom_call" | custom-call | tf_op jit(solution)/shard_map/mixer/pallas_call | solution.py:682
  60.5 0.0 copy-done
  60.5 1.7 %convolution_convert_fusion = bf16[256,2048]{1,0:T(8,128)(2,1)} fusion(bf16[256,512]{1,0:T(8,128)(2,1)S(1)} %mixer.1, bf16[512,2048]{1,0:T(8,128)(2,1)S(1)} %copy-done), kind=kOutput, calls=%fused_computation | convolution fusion | flops 537395200 | bytes 3407872 | tf_op jit(solution)/shard_map/dot_general | solution.py:746
Async XLA Ops:
  0.0 60.5 %copy-start = (bf16[512,2048]{1,0:T(8,128)(2,1)S(1)}, bf16[512,2048]{1,0:T(8,128)(2,1)}, u32[]{:S(2)}) copy-start(bf16[512,2048]{1,0:T(8,128)(2,1)} %param.19) | copy-start | bytes 6291460
